TPU v7x, 32 devices: a whole 2x2x4 slice. The times are simulated.
32 devices in a mesh: sp: 8 (over z, y), tp: 4 (over x, core).
Axes of the slice: x: 2, y: 2, z: 4, core: 2. Of those that a mesh axis runs over, the one named last changes fastest.
Arguments:
- tokens: bfloat16 [4096, 2048], P(('sp', 'tp')), may hold values from -6 to 6
- norm_gain: float32 [2048], replicated, may hold values from 0.25 to 5
- w_query_one: bfloat16 [2048, 512], P(None, 'tp'), may hold values from -0.21875 to 0.21875
- w_query_two: bfloat16 [2048, 512], P(None, 'tp'), may hold values from -0.21875 to 0.21875
- w_key_one: bfloat16 [2048, 512], P(None, 'tp'), may hold values from -0.125 to 0.125
- w_key_two: bfloat16 [2048, 512], P(None, 'tp'), may hold values from -0.125 to 0.125
- w_value: bfloat16 [2048, 1024], P(None, 'tp'), may hold values from -0.125 to 0.125
- mix_lambda: float32 [8], P('tp'), may hold values from 0.3 to 0.8
- head_gain: float32 [128], replicated, may hold values from 0.1 to 1.9
- w_ret_query: bfloat16 [2048, 512], P(None, 'tp'), may hold values from -0.125 to 0.125
- w_ret_key: bfloat16 [2048, 512], P(None, 'tp'), may hold values from -0.125 to 0.125
- w_ret_value: bfloat16 [2048, 1024], P(None, 'tp'), may hold values from -0.125 to 0.125
- retain_log: float32 [8, 4096], P('tp', 'sp'), may hold values from -1 to 0
- init_state: float32 [8, 64, 128], P('tp'), may hold values from -144 to 144
- w_out_diff: bfloat16 [1024, 2048], P('tp'), may hold values from -0.125 to 0.125
- w_out_ret: bfloat16 [1024, 2048], P('tp'), may hold values from -0.125 to 0.125
Outputs:
- mixed: bfloat16 [4096, 2048], P(('sp', 'tp'))
All inputs are finite; a program needn't handle non-finite values.
Results may differ from a plain program's by a relative error of at most 0.015.
The roundings to bfloat16 on the way count: a program that leaves them out, or rounds other values in their place, can miss the bound.
Values may be sent and summed in bfloat16 or wider, within the bound.
No kernel may reach another device: no remote copies, remote signals or barrier semaphores. Data moves between devices by JAX's collectives and lax.ppermute only.
A program may use at most 128 MiB of HBM per device.

v0:
```python
import functools
import math

import jax
import jax.numpy as jnp
from jax import lax
from jax.experimental import pallas as pl
from jax.experimental.pallas import tpu as pltpu
from jax.sharding import PartitionSpec as P


BLOCK = 256
NORM_EPS = 1e-06
HEAD_EPS = 1e-05
DIFF_SCALE = 0.8
HIGHEST = lax.Precision.HIGHEST
F32 = jnp.float32
BF16 = jnp.bfloat16
VMEM = pltpu.VMEM
SMEM = pltpu.SMEM
CORES = 2


def place(spans_low):
    s, t = lax.axis_index("sp"), lax.axis_index("tp")
    return t // CORES, lax.rem(s, spans_low), s // spans_low, lax.rem(t, CORES)


def whole(count):
    return [pl.BlockSpec(memory_space=VMEM)] * count


def project_kernel(heads, spans_low, *refs):
    sources, refs = refs[:11], refs[11:]
    targets, refs = refs[: heads + 1], refs[heads + 1 :]
    staged, refs = refs[: heads + 1], refs[heads + 1 :]
    rows_ref, (*landed, sem, out_sem) = refs[0], refs[1:]
    messages, ret_ref = staged[:heads], staged[heads]
    copies = [
        pltpu.make_async_copy(source, target, sem.at[n])
        for n, (source, target) in enumerate(zip(sources, landed))
    ]
    copies[10].start()
    for copy in copies[:10]:
        copy.start()
    _, _, z, c = place(spans_low)
    mine = sources[0].shape[0]
    copies[10].wait()
    for n, core in ((0, c), (1, CORES - 1 - c)):
        copies[n].wait()
        floats = landed[n][...].astype(F32)
        mean = jnp.mean(floats * floats, axis=-1, keepdims=True)
        rows_ref[pl.ds(pl.multiple_of(core * mine, mine), mine), :] = (
            floats * lax.rsqrt(mean + NORM_EPS) * landed[10][...]
        ).astype(BF16)
    k1, k2, v, q1, q2, rq, rk, rv = range(2, 10)
    rows = rows_ref.shape[0]
    width = sources[k1].shape[1]
    size = width // heads
    lane = lax.broadcasted_iota(jnp.int32, (rows, 2 * size), 1)
    low = lax.rem(z, heads)

    def product(*which):
        for n in which:
            copies[n].wait()
        parts = [landed[n][...] for n in which]
        w = parts[0] if len(parts) == 1 else jnp.concatenate(parts, axis=1)
        return jnp.dot(rows_ref[...], w, preferred_element_type=F32)

    def side(both, h):
        one, two = both[:, :width], both[:, width:]
        a = one if h == 0 else pltpu.roll(one, width - h * size, 1)
        shift = (size - h * size) % width
        b = two if shift == 0 else pltpu.roll(two, shift, 1)
        return jnp.where(lane < size, a[:, : 2 * size], b[:, : 2 * size]).astype(BF16)

    def deal(n, per_head):
        for r in range(heads):
            chosen = per_head[r]
            for h in range(heads):
                if h != r:
                    chosen = jnp.where(lax.rem(low + r, heads) == h, per_head[h], chosen)
            messages[r][n] = chosen

    keys = product(k1, k2)
    deal(0, [side(keys, h) for h in range(heads)])
    values = product(v)
    val = values.shape[1] // heads
    deal(1, [values[:, h * val : (h + 1) * val].astype(BF16) for h in range(heads)])
    queries = product(q1, q2)
    deal(2, [side(queries, h) for h in range(heads)])
    leaving = [
        pltpu.make_async_copy(source, target, out_sem.at[n])
        for n, (source, target) in enumerate(zip(staged, targets))
    ]
    for copy in leaving[:heads]:
        copy.start()
    ret_ref[:, : 2 * width] = product(rq, rk).astype(BF16)
    ret_ref[:, 2 * width :] = product(rv).astype(BF16)
    leaving[heads].start()
    for copy in leaving:
        copy.wait()


def project(block, partner, gain, weights, heads, val, spans_low):
    mine, width = block.shape
    rows = CORES * mine
    key = weights[0].shape[1]
    ret = sum(w.shape[1] for w in weights[5:])
    message = (3, rows, val)
    return pl.pallas_call(
        functools.partial(project_kernel, heads, spans_low),
        out_shape=[jax.ShapeDtypeStruct(message, BF16)] * heads
        + [jax.ShapeDtypeStruct((rows, ret), BF16)],
        in_specs=[pl.BlockSpec(memory_space=pltpu.HBM)] * (3 + len(weights)),
        out_specs=[pl.BlockSpec(memory_space=pltpu.HBM)] * (heads + 1),
        scratch_shapes=[VMEM(message, BF16)] * heads + [VMEM((rows, ret), BF16), VMEM((rows, width), BF16)]
        + [VMEM(a.shape, a.dtype) for a in (block, partner, *weights, gain)]
        + [pltpu.SemaphoreType.DMA((3 + len(weights),)), pltpu.SemaphoreType.DMA((heads + 1,))],
        compiler_params=pltpu.CompilerParams(vmem_limit_bytes=60 << 20),
        cost_estimate=pl.CostEstimate(
            flops=2 * rows * width * (6 * key + 2 * weights[4].shape[1]) * 2,
            bytes_accessed=0, transcendentals=0,
        ),
        name="project",
    )(block, partner, *weights, gain)


def attend(own, shared, lam, lam_other, gain, heads, halves, spans_low, sp):
    rows, val = own[0].shape[1], own[0].shape[2]
    group = halves if sp * halves * halves * rows * rows * 8 <= (24 << 20) else 1
    count = len(own) + len(shared)

    def kernel(*refs):
        own_refs, shared_refs = refs[: len(own)], refs[len(own) : count]
        lam_ref, other_ref, gain_ref = refs[count : count + 3]
        outs = refs[count + 3 : count + 3 + heads]
        kv_ref, q_ref, s_ref, m_ref, acc_ref, sem = refs[count + 3 + heads :]
        x, y, z, c = place(spans_low)
        j = lax.rem(z, heads)

        def span_of(r, b, d):
            low = lax.rem(j - r + heads, heads)
            core = lax.rem(c + d, CORES)
            high = lax.rem(core - low + CORES * heads, CORES)
            return (high * heads + low) * spans_low + lax.rem(y + b, spans_low)

        copies = []

        def fetch(source, target):
            copy = pltpu.make_async_copy(source, target, sem.at[len(copies)])
            copy.start()
            copies.append(copy)

        for p in range(halves):
            half = lax.rem(x + p, halves)
            for r in range(heads):
                fetch(own_refs[p * heads + r].at[pl.ds(0, 2)], kv_ref.at[span_of(r, 0, 0), half])
                fetch(own_refs[p * heads + r].at[2], q_ref.at[r, p])
        n = 0
        for b in range(spans_low):
            for d in range(CORES):
                if b == 0 and d == 0:
                    continue
                for p in range(halves):
                    for r in range(heads):
                        fetch(
                            shared_refs[n].at[r],
                            kv_ref.at[span_of(r, b, d), lax.rem(x + p, halves)],
                        )
                    n += 1
        for copy in copies:
            copy.wait()

        owner = z // heads
        lam = lam_ref[j]
        lam = jnp.where(c == owner, lam, other_ref[j])
        scale = (val // 2) ** (-0.5) * math.log2(math.e)
        lane = lax.broadcasted_iota(jnp.int32, (rows, val), 1)
        zero = jnp.zeros((rows, val), BF16)
        keys = halves * rows

        def part(r, first):
            span = span_of(r, 0, 0)
            queries = []
            for p in range(first, first + group):
                q = q_ref[r, p]
                queries += [jnp.where(lane < val // 2, q, zero), jnp.where(lane < val // 2, zero, q)]
            stack = jnp.concatenate(queries, axis=0)
            m_ref[...] = jnp.full(m_ref.shape, -jnp.inf, F32)

            def scores(at):
                pieces = kv_ref.at[at]
                k = jnp.concatenate([pieces[h, 0] for h in range(halves)], axis=0)
                return lax.dot_general(
                    stack, k, (((1,), (1,)), ((), ())), preferred_element_type=F32
                )

            def keep(at, s):
                s_ref[at] = s
                m = m_ref[...]
                for lanes in range(0, keys, 128):
                    m = jnp.maximum(m, s[:, lanes : lanes + 128])
                m_ref[...] = m

            def full(at, carry):
                keep(at, scores(at))
                return carry

            lax.fori_loop(0, span, full, 0)
            s = scores(span)
            at_key = lax.broadcasted_iota(jnp.int32, (rows, keys), 1)
            at_row = lax.broadcasted_iota(jnp.int32, (rows, keys), 0)
            masked = []
            for p in range(group):
                begin = lax.rem(x + first + p, halves) * rows
                for i in range(2):
                    at = (2 * p + i) * rows
                    masked.append(jnp.where(at_key <= at_row + begin, s[at : at + rows], -jnp.inf))
            keep(span, jnp.concatenate(masked, axis=0))
            m_ref[...] = jnp.broadcast_to(
                jnp.max(m_ref[...], axis=1, keepdims=True), m_ref.shape
            )
            acc_ref[...] = jnp.zeros_like(acc_ref)
            ones = jnp.ones((keys, val), BF16)

            def gather(at, carry):
                m = m_ref[...]
                s = s_ref[at]
                e = jnp.concatenate(
                    [
                        jnp.exp2((s[:, lanes : lanes + 128] - m) * scale).astype(BF16)
                        for lanes in range(0, keys, 128)
                    ],
                    axis=1,
                )
                pieces = kv_ref.at[at]
                v = jnp.concatenate([pieces[h, 1] for h in range(halves)], axis=0)
                acc_ref[...] += jnp.dot(
                    e, jnp.concatenate([v, ones], axis=1), preferred_element_type=F32
                )
                return carry

            lax.fori_loop(0, span + 1, gather, 0)
            for p in range(group):
                at = 2 * p * rows
                one, two = acc_ref[at : at + rows], acc_ref[at + rows : at + 2 * rows]
                attn = one[:, :val] / one[:, val:] - lam * (two[:, :val] / two[:, val:])
                mean = jnp.mean(attn * attn, axis=-1, keepdims=True)
                out = attn * lax.rsqrt(mean + HEAD_EPS) * gain_ref[...] * DIFF_SCALE
                outs[r][first + p] = out.astype(BF16)

        for r in range(heads):
            for first in range(0, halves, group):
                part(r, first)

    total = 2 * group * rows
    fetches = 2 * halves * heads + len(shared) * heads
    return pl.pallas_call(
        kernel,
        out_shape=[jax.ShapeDtypeStruct((halves, rows, val), BF16)] * heads,
        in_specs=[pl.BlockSpec(memory_space=pltpu.HBM)] * count
        + [pl.BlockSpec(memory_space=SMEM)] * 2 + whole(1),
        out_specs=whole(heads),
        scratch_shapes=[
            VMEM((sp, halves, 2, rows, val), BF16),
            VMEM((heads, halves, rows, val), BF16),
            VMEM((sp, total, halves * rows), F32),
            VMEM((total, 128), F32),
            VMEM((total, 2 * val), F32),
            pltpu.SemaphoreType.DMA((fetches,)),
        ],
        compiler_params=pltpu.CompilerParams(vmem_limit_bytes=60 * 1024 * 1024),
        cost_estimate=pl.CostEstimate(
            flops=heads * halves * rows * sp * rows * val * 16, bytes_accessed=0, transcendentals=0
        ),
        name="attend",
    )(*own, *shared, lam, lam_other, gain)


def running_log(logs, column):
    size = logs.shape[1]
    row = lax.broadcasted_iota(jnp.int32, (size, size), 0)
    col = lax.broadcasted_iota(jnp.int32, (size, size), 1)
    if column:
        upto = (col <= row).astype(F32)
        return lax.dot_general(
            upto, logs, (((1,), (1,)), ((), ())), precision=HIGHEST, preferred_element_type=F32
        )
    upto = (row <= col).astype(F32)
    return jnp.dot(logs, upto, precision=HIGHEST, preferred_element_type=F32)


def retention_states(slabs, logs, heads, key, val, spans_low):
    halves = len(slabs)
    rows, width = slabs[0].shape
    blocks = halves * rows // BLOCK

    def kernel(log_ref, *refs):
        slab_refs, (out_ref, u_ref, slab_ref) = refs[:halves], refs[halves:]
        x, _, _, _ = place(spans_low)
        for p in range(halves):
            begin = lax.rem(x + p, halves) * rows
            slab_ref[pl.ds(pl.multiple_of(begin, rows), rows), :] = slab_refs[p][...]
        for h in range(heads):
            state, total = None, None
            for n in range(blocks):
                at = slice(n * BLOCK, (n + 1) * BLOCK)
                k = slab_ref[at, (heads + h) * key : (heads + h + 1) * key].astype(F32)
                v = slab_ref[at, 2 * heads * key + h * val : 2 * heads * key + (h + 1) * val]
                logs = log_ref[h : h + 1, at]
                c_col = running_log(logs, True)
                last = jnp.sum(logs, axis=1, keepdims=True)
                kd = (k * key ** (-0.5) * jnp.exp(last - c_col)).astype(BF16)
                u = lax.dot_general(
                    kd, v, (((0,), (0,)), ((), ())), preferred_element_type=F32
                )
                u_ref[n, h] = u
                state = u if n == 0 else state * jnp.exp(last) + u
                total = last if n == 0 else total + last
            out_ref[h, :key] = state
            out_ref[h, key:] = jnp.broadcast_to(total, (8, val))

    return pl.pallas_call(
        kernel,
        out_shape=[
            jax.ShapeDtypeStruct((heads, key + 8, val), F32),
            jax.ShapeDtypeStruct((blocks, heads, key, val), F32),
        ],
        in_specs=whole(1 + halves),
        out_specs=whole(2),
        scratch_shapes=[VMEM((halves * rows, width), BF16)],
        cost_estimate=pl.CostEstimate(
            flops=2 * halves * rows * key * val * heads * 8, bytes_accessed=0, transcendentals=0
        ),
        name="states",
    )(logs, *slabs)


def retain(slabs, logs, parts, before, init, heads, key, val, spans_low):
    halves = len(slabs)
    rows, width = slabs[0].shape
    per_half = rows // BLOCK

    def kernel(log_ref, parts_ref, before_ref, init_ref, *refs):
        slab_refs, (out_ref, slab_ref) = refs[:halves], refs[halves:]
        x, _, _, _ = place(spans_low)
        for p in range(halves):
            begin = lax.rem(x + p, halves) * rows
            slab_ref[pl.ds(pl.multiple_of(begin, rows), rows), :] = slab_refs[p][...]
        at_row = lax.broadcasted_iota(jnp.int32, (BLOCK, BLOCK), 0)
        at_col = lax.broadcasted_iota(jnp.int32, (BLOCK, BLOCK), 1)
        for h in range(heads):
            state = before_ref[h, :key] + jnp.exp(before_ref[h, key : key + 1]) * init_ref[h]
            for n in range(halves * per_half):
                at = slice(n * BLOCK, (n + 1) * BLOCK)
                q = slab_ref[at, h * key : (h + 1) * key]
                k = slab_ref[at, (heads + h) * key : (heads + h + 1) * key]
                v = slab_ref[at, 2 * heads * key + h * val : 2 * heads * key + (h + 1) * val]
                logs = log_ref[h : h + 1, at]
                c_col = running_log(logs, True)
                c_row = running_log(logs, False)
                raw = lax.dot_general(q, k, (((1,), (1,)), ((), ())), preferred_element_type=F32)
                gap = jnp.where(at_row >= at_col, c_col - c_row, -jnp.inf)
                g = (raw * key ** (-0.5) * jnp.exp(gap)).astype(BF16)
                r = jnp.dot(g, v, preferred_element_type=F32)
                r += jnp.dot(
                    q.astype(F32) * jnp.exp(c_col), state,
                    precision=HIGHEST, preferred_element_type=F32,
                )
                mean = jnp.mean(r * r, axis=-1, keepdims=True)
                p = lax.rem(n // per_half - x + halves, halves)
                inside = slice((n % per_half) * BLOCK, (n % per_half + 1) * BLOCK)
                out_ref[p, inside, h * val : (h + 1) * val] = (
                    r * lax.rsqrt(mean + HEAD_EPS)
                ).astype(BF16)
                last = jnp.sum(logs, axis=1, keepdims=True)
                state = state * jnp.exp(last) + parts_ref[n, h]

    return pl.pallas_call(
        kernel,
        out_shape=jax.ShapeDtypeStruct((halves, rows, heads * val), BF16),
        in_specs=whole(4 + halves),
        out_specs=pl.BlockSpec(memory_space=VMEM),
        scratch_shapes=[VMEM((halves * rows, width), BF16)],
        cost_estimate=pl.CostEstimate(
            flops=2 * BLOCK * halves * rows * 1024, bytes_accessed=0, transcendentals=0
        ),
        name="retain",
    )(logs, parts, before, init, *slabs)


def on_device(
    sp, tp,
    tokens, norm_gain, w_query_one, w_query_two, w_key_one, w_key_two, w_value, mix_lambda,
    head_gain, w_ret_query, w_ret_key, w_ret_value, retain_log, init_state, w_out_diff, w_out_ret,
):
    heads = mix_lambda.shape[0]
    ret_heads = init_state.shape[0]
    key = init_state.shape[1]
    val = head_gain.shape[0]
    halves = tp // CORES
    spans_low = sp // (CORES * heads)
    axes = ("sp", "tp")

    def send(array, rule):
        pairs = []
        for s in range(sp):
            for t in range(tp):
                to = rule(s // spans_low, s % spans_low, t // CORES, t % CORES)
                pairs.append((s * tp + t, (to[0] * spans_low + to[1]) * tp + to[2] * CORES + to[3]))
        return lax.ppermute(array, axes, pairs)

    _, _, z, c = place(spans_low)
    s = lax.axis_index("sp")
    other_core = lambda z, y, x, c: (z, y, x, (c + 1) % CORES)

    weights = (
        w_key_one, w_key_two, w_value, w_query_one, w_query_two,
        w_ret_query, w_ret_key, w_ret_value,
    )
    blocks = [tokens] + [
        send(tokens, lambda z, y, x, c: (z, y, (x - p) % halves, c)) for p in range(1, halves)
    ]
    lam_other = send(mix_lambda, other_core)

    after = lambda value, event: lax.optimization_barrier((value, event))[0]

    def fetch(weight, event):
        return [weight] + [
            send(after(weight, event), lambda z, y, x, c: (z, y, (x - q) % halves, c))
            for q in range(1, halves)
        ]

    def spread(r):
        def rule(z, y, x, c):
            lo, hi = z % heads, z // heads
            return (c * heads + (lo + r) % heads, y, x, (hi + lo) % CORES)

        return rule

    def unspread(r):
        def rule(z, y, x, c):
            j = z % heads
            lo = (j - r) % heads
            hi = (c - lo) % CORES
            return (hi * heads + lo, y, x, z // heads)

        return rule

    own, slabs = [], []
    for block in blocks:
        block = after(block, slabs[-1]) if slabs else block
        partner = send(block, other_core)
        *messages, slab = project(
            block, partner, norm_gain[None, :], weights, heads, val, spans_low
        )
        own.append([send(message, spread(r)) for r, message in enumerate(messages)])
        slabs.append(slab)
    half_rows = slabs[0].shape[0]
    w_diff = fetch(w_out_diff, slabs[0])
    w_ret = fetch(w_out_ret, slabs[-1])

    shared, packs = {}, []
    for p in range(halves):
        arrived = own[p] if p == halves - 1 else after(own[p], slabs[p + 1])
        kv = jnp.stack([message[:2] for message in arrived])
        packs.append(kv)
        for b in range(spans_low):
            moved = kv if b == 0 else send(kv, lambda z, y, x, c: (z, (y - b) % spans_low, x, c))
            if b:
                shared[b, 0, p] = moved
            shared[b, 1, p] = send(moved, other_core)
    shared = [
        shared[b, d, p]
        for b in range(spans_low) for d in range(CORES) for p in range(halves) if b or d
    ]

    slabs = after(slabs, packs[0])
    local, parts = retention_states(slabs, retain_log, ret_heads, key, val, spans_low)
    before = jnp.zeros_like(local)
    is_state = lax.broadcasted_iota(jnp.int32, local.shape, 1) < key

    def join(first, second):
        return first * jnp.where(is_state, jnp.exp(second[:, key : key + 1]), 1.0) + second

    diff = attend(
        [message for half in own for message in half], shared, mix_lambda, lam_other,
        head_gain[None, :], heads, halves, spans_low, sp,
    )
    step = 1
    while step < sp:
        heard = lax.ppermute(local, "sp", [(i, i ^ step) for i in range(sp)])
        if step == 1:
            heard = after(heard, packs[-1])
        if 2 * step >= sp:
            heard = after(heard, diff)
        upper = (s // step) % 2 == 1
        before = jnp.where(upper, join(heard, before), before)
        local = jnp.where(upper, join(heard, local), join(local, heard))
        step *= 2
    ret_out = retain(slabs, retain_log, parts, before, init_state, ret_heads, key, val, spans_low)

    home = [send(diff[r], unspread(r)) for r in range(heads)]
    low = lax.rem(z, heads)
    by_head = []
    for h in range(heads):
        block = home[0]
        for r in range(1, heads):
            block = jnp.where(lax.rem(low + r, heads) == h, home[r], block)
        by_head.append(block)
    mine = half_rows // CORES
    across = lambda p: lambda z, y, x, c: (z, y, (x + p) % halves, c)
    rows_of = lambda a, core: lax.dynamic_slice_in_dim(a, core * mine, mine, 0)

    def product(a, w):
        return jnp.dot(a, w, preferred_element_type=F32)

    w_diff = [(w, send(after(w, packs[-1]), other_core)) for w in w_diff]
    w_ret = [(w, send(after(w, diff), other_core)) for w in w_ret]
    result = None
    for p in reversed(range(halves)):
        cols = jnp.concatenate([b[p] for b in by_head] + [ret_out[p]], axis=1)
        if p:
            cols = send(cols, across(p))
        theirs = send(rows_of(cols, 1 - c), other_core)
        q = (halves - p) % halves
        split = heads * val
        for core, rows in enumerate((rows_of(cols, c), theirs)):
            term = product(rows[:, :split], w_diff[q][core]) + product(rows[:, split:], w_ret[q][core])
            result = term if result is None else result + term
    return result.astype(BF16)


def solution(mesh):
    sp, tp = mesh.shape["sp"], mesh.shape["tp"]
    in_specs = (
        P(("sp", "tp"), None), P(),
        P(None, "tp"), P(None, "tp"), P(None, "tp"), P(None, "tp"), P(None, "tp"),
        P("tp"), P(),
        P(None, "tp"), P(None, "tp"), P(None, "tp"),
        P("tp", "sp"), P("tp", None, None), P("tp", None), P("tp", None),
    )

    def body(*args):
        return on_device(sp, tp, *args)

    return jax.shard_map(
        body, mesh=mesh, in_specs=in_specs, out_specs=P(("sp", "tp"), None), check_vma=False
    )
```

profile of v0, /device:TPU:0, one launch (start us, length us, event | category | flops | bytes accessed | tf_op | source)
XLA Modules:
  0.0 98.7 jit_solution(8475222143714648340)
XLA Ops:
  0.5 2.5 %collective-permute-start.3 = (bf16[128,2048]{1,0:T(8,128)(2,1)}, bf16[128,2048]{1,0:T(8,128)(2,1)S(1)}, u32[]{:S(2)}, u32[]{:S(2)}) collective-permute-start(bf16[128,2048]{1,0:T(8,128)(2,1)} %refs_0_.1), channel_id=1, source_target_pairs={{0,2},{1,3},{2,0},{3,1},{4,6},{5,7},{6,4},{7,5},{8,10},{9,11},{10,... | collective-permute-start | bytes 1572872 | tf_op jit(solution)/shard_map/ppermute | solution.py:412
  3.8 5.8 %project.2 = (bf16[3,256,128]{2,1,0:T(8,128)(2,1)}, bf16[3,256,128]{2,1,0:T(8,128)(2,1)}, bf16[256,512]{1,0:T(8,128)(2,1)}) custom-call(bf16[128,2048]{1,0:T(8,128)(2,1)} %refs_0_.1, bf16[128,2048]{1,0:T(8,128)(2,1)} %copy-done.10, bf16[2048,128]{1,0:T(8,128)(2,1)} %refs_2_.3, bf16[2048,128]{1,0:T(8,128)(2,1)} %refs_3_.3, bf16[2048,256]{1,0:T(8,128)(2,1)} %refs_4_.3, ...), custom_call_target="tpu_custom_call" | custom-call | flops 2147483648 | tf_op jit(solution)/shard_map/project/pallas_call | solution.py:111
  9.6 6.2 %collective-permute-done.3.refs_0_ = bf16[128,2048]{1,0:T(8,128)(2,1)S(1)} collective-permute-done((bf16[128,2048]{1,0:T(8,128)(2,1)}, bf16[128,2048]{1,0:T(8,128)(2,1)S(1)}, u32[]{:S(2)}, u32[]{:S(2)}) %collective-permute-start.3) | collective-permute-done | bytes 524320 | tf_op jit(solution)/shard_map/ppermute | solution.py:412
  15.8 1.6 %collective-permute-start.1 = (bf16[3,256,128]{2,1,0:T(8,128)(2,1)}, bf16[3,256,128]{2,1,0:T(8,128)(2,1)S(1)}, u32[]{:S(2)}, u32[]{:S(2)}) collective-permute-start(bf16[3,256,128]{2,1,0:T(8,128)(2,1)} %get-tuple-element.28), channel_id=1, source_target_pairs={{0,0},{1,16},{2,2},{3,18},{4,4},{5,20},{6,6},{7,22},{8,9},{9,25},{... | collective-permute-start | bytes 589832 | tf_op jit(solution)/shard_map/ppermute | solution.py:412
  17.4 2.7 %collective-permute-start.2 = (bf16[3,256,128]{2,1,0:T(8,128)(2,1)}, bf16[3,256,128]{2,1,0:T(8,128)(2,1)S(1)}, u32[]{:S(2)}, u32[]{:S(2)}) collective-permute-start(bf16[3,256,128]{2,1,0:T(8,128)(2,1)} %get-tuple-element.29), channel_id=1, source_target_pairs={{0,8},{1,24},{2,10},{3,26},{4,12},{5,28},{6,14},{7,30},{8,1},{9,17... | collective-permute-start | bytes 589832 | tf_op jit(solution)/shard_map/ppermute | solution.py:412
  20.1 1.5 %collective-permute-start.20 = (bf16[256,2048]{1,0:T(8,128)(2,1)S(1)}, bf16[256,2048]{1,0:T(8,128)(2,1)S(1)}, u32[]{:S(2)}, u32[]{:S(2)}) collective-permute-start(bf16[256,2048]{1,0:T(8,128)(2,1)S(1)} %copy-done), channel_id=1, source_target_pairs={{0,2},{1,3},{2,0},{3,1},{4,6},{5,7},{6,4},{7,5},{8,10},{9,11},{10,... | collective-permute-start | bytes 3145736 | tf_op jit(solution)/shard_map/ppermute | solution.py:412
  22.4 5.7 %project.3 = (bf16[3,256,128]{2,1,0:T(8,128)(2,1)}, bf16[3,256,128]{2,1,0:T(8,128)(2,1)}, bf16[256,512]{1,0:T(8,128)(2,1)}) custom-call(bf16[128,2048]{1,0:T(8,128)(2,1)} %copy-done.8, bf16[128,2048]{1,0:T(8,128)(2,1)} %copy-done.9, bf16[2048,128]{1,0:T(8,128)(2,1)} %refs_2_.3, bf16[2048,128]{1,0:T(8,128)(2,1)} %refs_3_.3, bf16[2048,256]{1,0:T(8,128)(2,1)} %refs_4_.3, ...), custom_call_target="tpu_custom_call" | custom-call | flops 2147483648 | tf_op jit(solution)/shard_map/project/pallas_call | solution.py:111
  28.1 1.7 %collective-permute-done.2.refs_1_ = bf16[3,256,128]{2,1,0:T(8,128)(2,1)S(1)} collective-permute-done((bf16[3,256,128]{2,1,0:T(8,128)(2,1)}, bf16[3,256,128]{2,1,0:T(8,128)(2,1)S(1)}, u32[]{:S(2)}, u32[]{:S(2)}) %collective-permute-start.2) | collective-permute-done | bytes 196640 | tf_op jit(solution)/shard_map/ppermute | solution.py:412
  30.6 1.7 %collective-permute-start.9 = (bf16[2,2,256,128]{3,2,1,0:T(8,128)(2,1)S(1)}, bf16[2,2,256,128]{3,2,1,0:T(8,128)(2,1)S(1)}, u32[]{:S(2)}, u32[]{:S(2)}) collective-permute-start(bf16[2,2,256,128]{3,2,1,0:T(8,128)(2,1)S(1)} %pad_maximum_fusion), channel_id=1, source_target_pairs={{0,4},{1,5},{2,6},{3,7},{4,0},{5,1},{6,2},{7,3},{8,12},{9,13},{10,... | collective-permute-start | bytes 786440 | tf_op jit(solution)/shard_map/ppermute | solution.py:412
  32.2 1.6 %collective-permute-start.6 = (bf16[3,256,128]{2,1,0:T(8,128)(2,1)S(1)}, bf16[3,256,128]{2,1,0:T(8,128)(2,1)S(1)}, u32[]{:S(2)}, u32[]{:S(2)}) collective-permute-start(bf16[3,256,128]{2,1,0:T(8,128)(2,1)S(1)} %copy-done.17), channel_id=1, source_target_pairs={{0,8},{1,24},{2,10},{3,26},{4,12},{5,28},{6,14},{7,30},{8,1},{9,17... | collective-permute-start | bytes 589832 | tf_op jit(solution)/shard_map/ppermute | solution.py:412
  33.8 2.3 %states.1 = (f32[2,72,128]{2,1,0:T(8,128)}, f32[2,2,64,128]{3,2,1,0:T(8,128)}) custom-call(f32[2,512]{1,0:T(2,128)} %log_ref.3, bf16[256,512]{1,0:T(8,128)(2,1)} %get-tuple-element.39.refs_0_, bf16[256,512]{1,0:T(8,128)(2,1)} %get-tuple-element.40.refs_1_), custom_call_target="tpu_custom_call" | custom-call | flops 134217728 | tf_op jit(solution)/shard_map/states/pallas_call | solution.py:324
  37.2 4.6 %collective-permute-done.6.refs_3_ = bf16[3,256,128]{2,1,0:T(8,128)(2,1)S(1)} collective-permute-done((bf16[3,256,128]{2,1,0:T(8,128)(2,1)S(1)}, bf16[3,256,128]{2,1,0:T(8,128)(2,1)S(1)}, u32[]{:S(2)}, u32[]{:S(2)}) %collective-permute-start.6) | collective-permute-done | bytes 196640 | tf_op jit(solution)/shard_map/ppermute | solution.py:412
  41.8 1.6 %collective-permute-start.5 = (bf16[3,256,128]{2,1,0:T(8,128)(2,1)}, bf16[3,256,128]{2,1,0:T(8,128)(2,1)S(1)}, u32[]{:S(2)}, u32[]{:S(2)}) collective-permute-start(bf16[3,256,128]{2,1,0:T(8,128)(2,1)} %get-tuple-element.32), channel_id=1, source_target_pairs={{0,0},{1,16},{2,2},{3,18},{4,4},{5,20},{6,6},{7,22},{8,9},{9,25},{... | collective-permute-start | bytes 589832 | tf_op jit(solution)/shard_map/ppermute | solution.py:412
  44.8 6.6 %collective-permute-start.17 = (f32[2,72,128]{2,1,0:T(8,128)S(1)}, f32[2,72,128]{2,1,0:T(8,128)S(1)}, u32[]{:S(2)}, u32[]{:S(2)}) collective-permute-start(f32[2,72,128]{2,1,0:T(8,128)S(1)} %get-tuple-element.61), channel_id=1, source_target_pairs={{0,8},{4,12},{8,0},{12,4},{16,24},{20,28},{24,16},{28,20},{1,9},{5... | collective-permute-start | bytes 221192 | tf_op jit(solution)/shard_map/ppermute | solution.py:493
  51.5 2.2 %collective-permute-done.17 = f32[2,72,128]{2,1,0:T(8,128)S(1)} collective-permute-done((f32[2,72,128]{2,1,0:T(8,128)S(1)}, f32[2,72,128]{2,1,0:T(8,128)S(1)}, u32[]{:S(2)}, u32[]{:S(2)}) %collective-permute-start.17) | collective-permute-done | bytes 73760 | tf_op jit(solution)/shard_map/ppermute | solution.py:493
  54.4 1.6 %collective-permute-start.12 = (bf16[2,2,256,128]{3,2,1,0:T(8,128)(2,1)S(1)}, bf16[2,2,256,128]{3,2,1,0:T(8,128)(2,1)S(1)}, u32[]{:S(2)}, u32[]{:S(2)}) collective-permute-start(bf16[2,2,256,128]{3,2,1,0:T(8,128)(2,1)S(1)} %collective-permute-done.10.refs_7_), channel_id=1, source_target_pairs={{0,1},{1,0},{2,3},{3,2},{4,5},{5,4},{6,7},{7,6},{8,9},{9,8},{10,11... | collective-permute-start | bytes 786440 | tf_op jit(solution)/shard_map/ppermute | solution.py:412
  59.5 1.8 %collective-permute-start.18 = (f32[2,72,128]{2,1,0:T(8,128)S(1)}, f32[2,72,128]{2,1,0:T(8,128)S(1)}, u32[]{:S(2)}, u32[]{:S(2)}) collective-permute-start(f32[2,72,128]{2,1,0:T(8,128)S(1)} %get-tuple-element.59), channel_id=1, source_target_pairs={{0,16},{4,20},{8,24},{12,28},{16,0},{20,4},{24,8},{28,12},{1,17},{... | collective-permute-start | bytes 221192 | tf_op jit(solution)/shard_map/ppermute | solution.py:493
  62.8 11.2 %attend.1 = (bf16[2,256,128]{2,1,0:T(8,128)(2,1)}, bf16[2,256,128]{2,1,0:T(8,128)(2,1)}) custom-call(bf16[3,256,128]{2,1,0:T(8,128)(2,1)} %copy-done.5, bf16[3,256,128]{2,1,0:T(8,128)(2,1)} %copy-done.6, bf16[3,256,128]{2,1,0:T(8,128)(2,1)} %copy-done.4, bf16[3,256,128]{2,1,0:T(8,128)(2,1)} %copy-done.3, bf16[2,2,256,128]{3,2,1,0:T(8,128)(2,1)} %copy-done.12, ...), custom_call_target="tpu_custom_call" | custom-call | flops 4294967296 | tf_op jit(solution)/shard_map/attend/pallas_call | solution.py:259
  73.9 2.2 %collective-permute-start.14 = (bf16[2,256,128]{2,1,0:T(8,128)(2,1)}, bf16[2,256,128]{2,1,0:T(8,128)(2,1)S(1)}, u32[]{:S(2)}, u32[]{:S(2)}) collective-permute-start(bf16[2,256,128]{2,1,0:T(8,128)(2,1)} %get-tuple-element.37), channel_id=1, source_target_pairs={{0,24},{1,8},{2,26},{3,10},{4,28},{5,12},{6,30},{7,14},{8,0},{9,16... | collective-permute-start | bytes 393224 | tf_op jit(solution)/shard_map/ppermute | solution.py:412
  76.1 1.6 %collective-permute-start.15 = (bf16[2,256,128]{2,1,0:T(8,128)(2,1)}, bf16[2,256,128]{2,1,0:T(8,128)(2,1)S(1)}, u32[]{:S(2)}, u32[]{:S(2)}) collective-permute-start(bf16[2,256,128]{2,1,0:T(8,128)(2,1)} %get-tuple-element.38), channel_id=1, source_target_pairs={{0,0},{1,16},{2,2},{3,18},{4,4},{5,20},{6,6},{7,22},{8,24},{9,8},{... | collective-permute-start | bytes 393224 | tf_op jit(solution)/shard_map/ppermute | solution.py:412
  78.4 3.7 %retain.1 = bf16[2,256,256]{2,1,0:T(8,128)(2,1)} custom-call(f32[2,512]{1,0:T(2,128)} %log_ref.3, f32[2,2,64,128]{3,2,1,0:T(8,128)} %get-tuple-element.41.parts_ref, f32[2,72,128]{2,1,0:T(8,128)} %add_select_fusion.before_ref, f32[2,64,128]{2,1,0:T(8,128)} %init_ref.1, bf16[256,512]{1,0:T(8,128)(2,1)} %get-tuple-element.39.refs_0_, ...), custom_call_target="tpu_custom_call" | custom-call | flops 268435456 | tf_op jit(solution)/shard_map/retain/pallas_call | solution.py:380
  85.3 1.5 %convolution_add_fusion.1 = f32[128,2048]{1,0:T(8,128)S(1)} fusion(f32[128,2048]{1,0:T(8,128)S(1)} %fusion.8, bf16[256,2048]{1,0:T(8,128)(2,1)} %param.31, bf16[256,512]{1,0:T(8,128)(2,1)S(1)} %pad_maximum_fusion.3, s32[]{:T(128)S(6)} %select_n.118, s32[]{:T(128)S(6)} %add.83), kind=kOutput, calls=%fused_computation.2 | convolution fusion | flops 134479872 | bytes 3211272 | tf_op jit(solution)/shard_map/dot_general | solution.py:517
  86.9 5.7 %collective-permute-done.19 = bf16[256,512]{1,0:T(8,128)(2,1)S(1)} collective-permute-done((bf16[256,512]{1,0:T(8,128)(2,1)S(1)}, bf16[256,512]{1,0:T(8,128)(2,1)S(1)}, u32[]{:S(2)}, u32[]{:S(2)}) %collective-permute-start.19) | collective-permute-done | bytes 262176 | tf_op jit(solution)/shard_map/ppermute | solution.py:412
  92.5 1.5 %fusion.13 = f32[128,2048]{1,0:T(8,128)S(1)} fusion(bf16[256,2048]{1,0:T(8,128)(2,1)} %collective-permute-done.21, bf16[256,512]{1,0:T(8,128)(2,1)S(1)} %collective-permute-done.19, s32[]{:T(128)S(6)} %select_n.118, s32[]{:T(128)S(6)} %add.83), kind=kOutput, calls=%fused_computation.35 | convolution fusion | flops 134217728 | bytes 2162696 | tf_op jit(solution)/shard_map/dot_general | solution.py:517
  (108 shorter events, 19.3 us)
Async XLA Ops:
  0.0 3.0 %collective-permute-start = (bf16[128,2048]{1,0:T(8,128)(2,1)}, bf16[128,2048]{1,0:T(8,128)(2,1)S(1)}, u32[]{:S(2)}, u32[]{:S(2)}) collective-permute-start(bf16[128,2048]{1,0:T(8,128)(2,1)} %refs_0_.1), channel_id=1, source_target_pairs={{0,1},{1,0},{2,3},{3,2},{4,5},{5,4},{6,7},{7,6},{8,9},{9,8},{10,11... | collective-permute-start | bytes 1572872 | tf_op jit(solution)/shard_map/ppermute | solution.py:412
  0.5 15.3 %collective-permute-start.3 = (bf16[128,2048]{1,0:T(8,128)(2,1)}, bf16[128,2048]{1,0:T(8,128)(2,1)S(1)}, u32[]{:S(2)}, u32[]{:S(2)}) collective-permute-start(bf16[128,2048]{1,0:T(8,128)(2,1)} %refs_0_.1), channel_id=1, source_target_pairs={{0,2},{1,3},{2,0},{3,1},{4,6},{5,7},{6,4},{7,5},{8,10},{9,11},{10,... | collective-permute-start | bytes 1572872 | tf_op jit(solution)/shard_map/ppermute | solution.py:412
  15.8 5.8 %collective-permute-start.4 = (bf16[128,2048]{1,0:T(8,128)(2,1)S(1)}, bf16[128,2048]{1,0:T(8,128)(2,1)S(1)}, u32[]{:S(2)}, u32[]{:S(2)}) collective-permute-start(bf16[128,2048]{1,0:T(8,128)(2,1)S(1)} %collective-permute-done.3.refs_0_), channel_id=1, source_target_pairs={{0,1},{1,0},{2,3},{3,2},{4,5},{5,4},{6,7},{7,6},{8,9},{9,8},{10,11... | collective-permute-start | bytes 1572872 | tf_op jit(solution)/shard_map/ppermute | solution.py:412
  15.8 12.3 %collective-permute-start.1 = (bf16[3,256,128]{2,1,0:T(8,128)(2,1)}, bf16[3,256,128]{2,1,0:T(8,128)(2,1)S(1)}, u32[]{:S(2)}, u32[]{:S(2)}) collective-permute-start(bf16[3,256,128]{2,1,0:T(8,128)(2,1)} %get-tuple-element.28), channel_id=1, source_target_pairs={{0,0},{1,16},{2,2},{3,18},{4,4},{5,20},{6,6},{7,22},{8,9},{9,25},{... | collective-permute-start | bytes 589832 | tf_op jit(solution)/shard_map/ppermute | solution.py:412
  17.4 12.5 %collective-permute-start.2 = (bf16[3,256,128]{2,1,0:T(8,128)(2,1)}, bf16[3,256,128]{2,1,0:T(8,128)(2,1)S(1)}, u32[]{:S(2)}, u32[]{:S(2)}) collective-permute-start(bf16[3,256,128]{2,1,0:T(8,128)(2,1)} %get-tuple-element.29), channel_id=1, source_target_pairs={{0,8},{1,24},{2,10},{3,26},{4,12},{5,28},{6,14},{7,30},{8,1},{9,17... | collective-permute-start | bytes 589832 | tf_op jit(solution)/shard_map/ppermute | solution.py:412
  20.1 36.0 %collective-permute-start.20 = (bf16[256,2048]{1,0:T(8,128)(2,1)S(1)}, bf16[256,2048]{1,0:T(8,128)(2,1)S(1)}, u32[]{:S(2)}, u32[]{:S(2)}) collective-permute-start(bf16[256,2048]{1,0:T(8,128)(2,1)S(1)} %copy-done), channel_id=1, source_target_pairs={{0,2},{1,3},{2,0},{3,1},{4,6},{5,7},{6,4},{7,5},{8,10},{9,11},{10,... | collective-permute-start | bytes 3145736 | tf_op jit(solution)/shard_map/ppermute | solution.py:412
  30.6 20.8 %collective-permute-start.9 = (bf16[2,2,256,128]{3,2,1,0:T(8,128)(2,1)S(1)}, bf16[2,2,256,128]{3,2,1,0:T(8,128)(2,1)S(1)}, u32[]{:S(2)}, u32[]{:S(2)}) collective-permute-start(bf16[2,2,256,128]{3,2,1,0:T(8,128)(2,1)S(1)} %pad_maximum_fusion), channel_id=1, source_target_pairs={{0,4},{1,5},{2,6},{3,7},{4,0},{5,1},{6,2},{7,3},{8,12},{9,13},{10,... | collective-permute-start | bytes 786440 | tf_op jit(solution)/shard_map/ppermute | solution.py:412
  32.2 27.2 %collective-permute-start.7 = (bf16[2,2,256,128]{3,2,1,0:T(8,128)(2,1)S(1)}, bf16[2,2,256,128]{3,2,1,0:T(8,128)(2,1)S(1)}, u32[]{:S(2)}, u32[]{:S(2)}) collective-permute-start(bf16[2,2,256,128]{3,2,1,0:T(8,128)(2,1)S(1)} %pad_maximum_fusion), channel_id=1, source_target_pairs={{0,1},{1,0},{2,3},{3,2},{4,5},{5,4},{6,7},{7,6},{8,9},{9,8},{10,11... | collective-permute-start | bytes 786440 | tf_op jit(solution)/shard_map/ppermute | solution.py:412
  32.2 9.5 %collective-permute-start.6 = (bf16[3,256,128]{2,1,0:T(8,128)(2,1)S(1)}, bf16[3,256,128]{2,1,0:T(8,128)(2,1)S(1)}, u32[]{:S(2)}, u32[]{:S(2)}) collective-permute-start(bf16[3,256,128]{2,1,0:T(8,128)(2,1)S(1)} %copy-done.17), channel_id=1, source_target_pairs={{0,8},{1,24},{2,10},{3,26},{4,12},{5,28},{6,14},{7,30},{8,1},{9,17... | collective-permute-start | bytes 589832 | tf_op jit(solution)/shard_map/ppermute | solution.py:412
  36.1 8.6 %collective-permute-start.16 = (f32[2,72,128]{2,1,0:T(8,128)}, f32[2,72,128]{2,1,0:T(8,128)S(1)}, u32[]{:S(2)}, u32[]{:S(2)}) collective-permute-start(f32[2,72,128]{2,1,0:T(8,128)} %get-tuple-element.42), channel_id=1, source_target_pairs={{0,4},{4,0},{8,12},{12,8},{16,20},{20,16},{24,28},{28,24},{1,5},{5... | collective-permute-start | bytes 221192 | tf_op jit(solution)/shard_map/ppermute | solution.py:493
  44.1 10.3 %collective-permute-start.10 = (bf16[2,2,256,128]{3,2,1,0:T(8,128)(2,1)S(1)}, bf16[2,2,256,128]{3,2,1,0:T(8,128)(2,1)S(1)}, u32[]{:S(2)}, u32[]{:S(2)}) collective-permute-start(bf16[2,2,256,128]{3,2,1,0:T(8,128)(2,1)S(1)} %pad_maximum_fusion.1), channel_id=1, source_target_pairs={{0,4},{1,5},{2,6},{3,7},{4,0},{5,1},{6,2},{7,3},{8,12},{9,13},{10,... | collective-permute-start | bytes 786440 | tf_op jit(solution)/shard_map/ppermute | solution.py:412
  44.8 8.9 %collective-permute-start.17 = (f32[2,72,128]{2,1,0:T(8,128)S(1)}, f32[2,72,128]{2,1,0:T(8,128)S(1)}, u32[]{:S(2)}, u32[]{:S(2)}) collective-permute-start(f32[2,72,128]{2,1,0:T(8,128)S(1)} %get-tuple-element.61), channel_id=1, source_target_pairs={{0,8},{4,12},{8,0},{12,4},{16,24},{20,28},{24,16},{28,20},{1,9},{5... | collective-permute-start | bytes 221192 | tf_op jit(solution)/shard_map/ppermute | solution.py:493
  51.4 8.1 %collective-permute-start.8 = (bf16[2,2,256,128]{3,2,1,0:T(8,128)(2,1)S(1)}, bf16[2,2,256,128]{3,2,1,0:T(8,128)(2,1)S(1)}, u32[]{:S(2)}, u32[]{:S(2)}) collective-permute-start(bf16[2,2,256,128]{3,2,1,0:T(8,128)(2,1)S(1)} %pad_maximum_fusion.1), channel_id=1, source_target_pairs={{0,1},{1,0},{2,3},{3,2},{4,5},{5,4},{6,7},{7,6},{8,9},{9,8},{10,11... | collective-permute-start | bytes 786440 | tf_op jit(solution)/shard_map/ppermute | solution.py:412
  53.7 7.7 %collective-permute-start.11 = (bf16[2,2,256,128]{3,2,1,0:T(8,128)(2,1)S(1)}, bf16[2,2,256,128]{3,2,1,0:T(8,128)(2,1)S(1)}, u32[]{:S(2)}, u32[]{:S(2)}) collective-permute-start(bf16[2,2,256,128]{3,2,1,0:T(8,128)(2,1)S(1)} %collective-permute-done.9.refs_6_), channel_id=1, source_target_pairs={{0,1},{1,0},{2,3},{3,2},{4,5},{5,4},{6,7},{7,6},{8,9},{9,8},{10,11... | collective-permute-start | bytes 786440 | tf_op jit(solution)/shard_map/ppermute | solution.py:412
  54.4 7.2 %collective-permute-start.12 = (bf16[2,2,256,128]{3,2,1,0:T(8,128)(2,1)S(1)}, bf16[2,2,256,128]{3,2,1,0:T(8,128)(2,1)S(1)}, u32[]{:S(2)}, u32[]{:S(2)}) collective-permute-start(bf16[2,2,256,128]{3,2,1,0:T(8,128)(2,1)S(1)} %collective-permute-done.10.refs_7_), channel_id=1, source_target_pairs={{0,1},{1,0},{2,3},{3,2},{4,5},{5,4},{6,7},{7,6},{8,9},{9,8},{10,11... | collective-permute-start | bytes 786440 | tf_op jit(solution)/shard_map/ppermute | solution.py:412
  57.9 27.3 %collective-permute-start.21 = (bf16[256,2048]{1,0:T(8,128)(2,1)}, bf16[256,2048]{1,0:T(8,128)(2,1)}, u32[]{:S(2)}, u32[]{:S(2)}) collective-permute-start(bf16[256,2048]{1,0:T(8,128)(2,1)} %param.31), channel_id=1, source_target_pairs={{0,2},{1,3},{2,0},{3,1},{4,6},{5,7},{6,4},{7,5},{8,10},{9,11},{10,... | collective-permute-start | bytes 3145736 | tf_op jit(solution)/shard_map/ppermute | solution.py:412
  59.4 38.1 %collective-permute-start.26 = (bf16[256,2048]{1,0:T(8,128)(2,1)S(1)}, bf16[256,2048]{1,0:T(8,128)(2,1)S(1)}, u32[]{:S(2)}, u32[]{:S(2)}) collective-permute-start(bf16[256,2048]{1,0:T(8,128)(2,1)S(1)} %copy-done), channel_id=1, source_target_pairs={{0,1},{1,0},{2,3},{3,2},{4,5},{5,4},{6,7},{7,6},{8,9},{9,8},{10,11... | collective-permute-start | bytes 3145736 | tf_op jit(solution)/shard_map/ppermute | solution.py:412
  59.5 16.6 %collective-permute-start.18 = (f32[2,72,128]{2,1,0:T(8,128)S(1)}, f32[2,72,128]{2,1,0:T(8,128)S(1)}, u32[]{:S(2)}, u32[]{:S(2)}) collective-permute-start(f32[2,72,128]{2,1,0:T(8,128)S(1)} %get-tuple-element.59), channel_id=1, source_target_pairs={{0,16},{4,20},{8,24},{12,28},{16,0},{20,4},{24,8},{28,12},{1,17},{... | collective-permute-start | bytes 221192 | tf_op jit(solution)/shard_map/ppermute | solution.py:493
  61.4 34.7 %collective-permute-start.23 = (bf16[256,2048]{1,0:T(8,128)(2,1)}, bf16[256,2048]{1,0:T(8,128)(2,1)S(1)}, u32[]{:S(2)}, u32[]{:S(2)}) collective-permute-start(bf16[256,2048]{1,0:T(8,128)(2,1)} %copy-done.1), channel_id=1, source_target_pairs={{0,1},{1,0},{2,3},{3,2},{4,5},{5,4},{6,7},{7,6},{8,9},{9,8},{10,11... | collective-permute-start | bytes 3145736 | tf_op jit(solution)/shard_map/ppermute | solution.py:412
  73.9 9.2 %collective-permute-start.14 = (bf16[2,256,128]{2,1,0:T(8,128)(2,1)}, bf16[2,256,128]{2,1,0:T(8,128)(2,1)S(1)}, u32[]{:S(2)}, u32[]{:S(2)}) collective-permute-start(bf16[2,256,128]{2,1,0:T(8,128)(2,1)} %get-tuple-element.37), channel_id=1, source_target_pairs={{0,24},{1,8},{2,26},{3,10},{4,28},{5,12},{6,30},{7,14},{8,0},{9,16... | collective-permute-start | bytes 393224 | tf_op jit(solution)/shard_map/ppermute | solution.py:412
  76.1 8.0 %collective-permute-start.15 = (bf16[2,256,128]{2,1,0:T(8,128)(2,1)}, bf16[2,256,128]{2,1,0:T(8,128)(2,1)S(1)}, u32[]{:S(2)}, u32[]{:S(2)}) collective-permute-start(bf16[2,256,128]{2,1,0:T(8,128)(2,1)} %get-tuple-element.38), channel_id=1, source_target_pairs={{0,0},{1,16},{2,2},{3,18},{4,4},{5,20},{6,6},{7,22},{8,24},{9,8},{... | collective-permute-start | bytes 393224 | tf_op jit(solution)/shard_map/ppermute | solution.py:412
  83.1 11.6 %collective-permute-start.27 = (bf16[256,2048]{1,0:T(8,128)(2,1)}, bf16[256,2048]{1,0:T(8,128)(2,1)S(1)}, u32[]{:S(2)}, u32[]{:S(2)}) collective-permute-start(bf16[256,2048]{1,0:T(8,128)(2,1)} %param.31), channel_id=1, source_target_pairs={{0,1},{1,0},{2,3},{3,2},{4,5},{5,4},{6,7},{7,6},{8,9},{9,8},{10,11... | collective-permute-start | bytes 3145736 | tf_op jit(solution)/shard_map/ppermute | solution.py:412
  84.2 8.3 %collective-permute-start.19 = (bf16[256,512]{1,0:T(8,128)(2,1)S(1)}, bf16[256,512]{1,0:T(8,128)(2,1)S(1)}, u32[]{:S(2)}, u32[]{:S(2)}) collective-permute-start(bf16[256,512]{1,0:T(8,128)(2,1)S(1)} %pad_maximum_fusion.2), channel_id=1, source_target_pairs={{0,2},{1,3},{2,0},{3,1},{4,6},{5,7},{6,4},{7,5},{8,10},{9,11},{10,... | collective-permute-start | bytes 786440 | tf_op jit(solution)/shard_map/ppermute | solution.py:412
  85.2 10.5 %collective-permute-start.24 = (bf16[256,2048]{1,0:T(8,128)(2,1)}, bf16[256,2048]{1,0:T(8,128)(2,1)S(1)}, u32[]{:S(2)}, u32[]{:S(2)}) collective-permute-start(bf16[256,2048]{1,0:T(8,128)(2,1)} %collective-permute-done.21), channel_id=1, source_target_pairs={{0,1},{1,0},{2,3},{3,2},{4,5},{5,4},{6,7},{7,6},{8,9},{9,8},{10,11... | collective-permute-start | bytes 3145736 | tf_op jit(solution)/shard_map/ppermute | solution.py:412
  (24 other events, 65.6 us)
where the time goes:
time: 99.6 us; the launch traced here: 98.7 us
  starting transfers between devices  33.1 us (33%)
  Pallas kernels  28.7 us (29%)
  waiting for transfers between devices  22.3 us (22%)
  local copies, waits for them, and re-layouts  7.43 us (7%)
  matrix products  5.74 us (6%)
  other arithmetic  1.02 us (1%)
    ppermute x25, starting transfers between devices, send(): return lax.ppermute(array, axes, pairs)  24.4 us
    ppermute x25, waiting for transfers between devices, send(): return lax.ppermute(array, axes, pairs)  20.1 us
    pallas_call x2, Pallas kernels, project(): pl.pallas_call(functools.partial(project_kernel, heads, spans_low), out_s...  11.5 us
    pallas_call x1, Pallas kernels, attend(): pl.pallas_call(kernel, out_shape=[jax.ShapeDtypeStruct((halves, rows, val...  11.2 us
    ppermute x3, starting transfers between devices, on_device(): heard = lax.ppermute(local, 'sp', [(i, i ^ step) for i in range(sp)])  8.75 us
    dot_general x8, matrix products, product(): return jnp.dot(a, w, preferred_element_type=F32)  5.74 us
    unnamed x40, local copies, waits for them, and re-layouts  5.59 us
    pallas_call x1, Pallas kernels, retain(): pl.pallas_call(kernel, out_shape=jax.ShapeDtypeStruct((halves, rows, head...  3.74 us
  transfers between devices with their start and end apart: 28, of which 7 were waited for; matrix products, arithmetic and copies ran while one was open for 8% of the time, Pallas kernels for 29%

commit v1 on v0

--- a/solution.py
+++ b/solution.py
@@ -145,18 +145,28 @@
             high = lax.rem(core - low + CORES * heads, CORES)
             return (high * heads + low) * spans_low + lax.rem(y + b, spans_low)
 
-        copies = []
-
-        def fetch(source, target):
-            copy = pltpu.make_async_copy(source, target, sem.at[len(copies)])
-            copy.start()
-            copies.append(copy)
+        asked = []
+
+        def fetch(source, span, half):
+            at = span * halves + half
+            pltpu.make_async_copy(source, kv_ref.at[span, half], sem.at[at]).start()
+
+        def arrive(span):
+            for half in range(halves):
+                pltpu.make_async_copy(
+                    kv_ref.at[span, half], kv_ref.at[span, half], sem.at[span * halves + half]
+                ).wait()
 
         for p in range(halves):
             half = lax.rem(x + p, halves)
             for r in range(heads):
-                fetch(own_refs[p * heads + r].at[pl.ds(0, 2)], kv_ref.at[span_of(r, 0, 0), half])
-                fetch(own_refs[p * heads + r].at[2], q_ref.at[r, p])
+                copy = pltpu.make_async_copy(
+                    own_refs[p * heads + r].at[2], q_ref.at[r, p],
+                    sem.at[sp * halves + p * heads + r],
+                )
+                copy.start()
+                asked.append(copy)
+                fetch(own_refs[p * heads + r].at[pl.ds(0, 2)], span_of(r, 0, 0), half)
         n = 0
         for b in range(spans_low):
             for d in range(CORES):
@@ -164,12 +174,9 @@
                     continue
                 for p in range(halves):
                     for r in range(heads):
-                        fetch(
-                            shared_refs[n].at[r],
-                            kv_ref.at[span_of(r, b, d), lax.rem(x + p, halves)],
-                        )
+                        fetch(shared_refs[n].at[r], span_of(r, b, d), lax.rem(x + p, halves))
                     n += 1
-        for copy in copies:
+        for copy in asked:
             copy.wait()
 
         owner = z // heads
@@ -192,7 +199,7 @@
             def scores(at):
                 pieces = kv_ref.at[at]
                 k = jnp.concatenate([pieces[h, 0] for h in range(halves)], axis=0)
-                return lax.dot_general(
+                return scale * lax.dot_general(
                     stack, k, (((1,), (1,)), ((), ())), preferred_element_type=F32
                 )
 
@@ -203,11 +210,21 @@
                     m = jnp.maximum(m, s[:, lanes : lanes + 128])
                 m_ref[...] = m
 
+            opening = r == 0 and first == 0
+
             def full(at, carry):
+                if opening:
+                    arrive(at)
                 keep(at, scores(at))
                 return carry
 
+            def rest(at, carry):
+                arrive(at)
+                return carry
+
             lax.fori_loop(0, span, full, 0)
+            if opening:
+                lax.fori_loop(span, sp, rest, 0)
             s = scores(span)
             at_key = lax.broadcasted_iota(jnp.int32, (rows, keys), 1)
             at_row = lax.broadcasted_iota(jnp.int32, (rows, keys), 0)
@@ -229,7 +246,7 @@
                 s = s_ref[at]
                 e = jnp.concatenate(
                     [
-                        jnp.exp2((s[:, lanes : lanes + 128] - m) * scale).astype(BF16)
+                        jnp.exp2(s[:, lanes : lanes + 128] - m).astype(BF16)
                         for lanes in range(0, keys, 128)
                     ],
                     axis=1,
@@ -255,7 +272,7 @@
                 part(r, first)
 
     total = 2 * group * rows
-    fetches = 2 * halves * heads + len(shared) * heads
+    fetches = sp * halves + halves * heads
     return pl.pallas_call(
         kernel,
         out_shape=[jax.ShapeDtypeStruct((halves, rows, val), BF16)] * heads,
@@ -270,7 +287,9 @@
             VMEM((total, 2 * val), F32),
             pltpu.SemaphoreType.DMA((fetches,)),
         ],
-        compiler_params=pltpu.CompilerParams(vmem_limit_bytes=60 * 1024 * 1024),
+        compiler_params=pltpu.CompilerParams(
+            vmem_limit_bytes=min(60 << 20, (12 << 20) + sp * rows * halves * (total + val) * 4)
+        ),
         cost_estimate=pl.CostEstimate(
             flops=heads * halves * rows * sp * rows * val * 16, bytes_accessed=0, transcendentals=0
         ),
@@ -278,17 +297,22 @@
     )(*own, *shared, lam, lam_other, gain)
 
 
-def running_log(logs, column):
-    size = logs.shape[1]
-    row = lax.broadcasted_iota(jnp.int32, (size, size), 0)
-    col = lax.broadcasted_iota(jnp.int32, (size, size), 1)
-    if column:
-        upto = (col <= row).astype(F32)
-        return lax.dot_general(
-            upto, logs, (((1,), (1,)), ((), ())), precision=HIGHEST, preferred_element_type=F32
-        )
-    upto = (row <= col).astype(F32)
-    return jnp.dot(logs, upto, precision=HIGHEST, preferred_element_type=F32)
+def running_logs(log_ref, heads, blocks, rows_too):
+    logs = jnp.concatenate(
+        [log_ref[h : h + 1, n * BLOCK : (n + 1) * BLOCK] for h in range(heads) for n in range(blocks)],
+        axis=0,
+    )
+    row = lax.broadcasted_iota(jnp.int32, (BLOCK, BLOCK), 0)
+    col = lax.broadcasted_iota(jnp.int32, (BLOCK, BLOCK), 1)
+    columns = lax.dot_general(
+        (col <= row).astype(F32), logs, (((1,), (1,)), ((), ())),
+        precision=HIGHEST, preferred_element_type=F32,
+    )
+    if not rows_too:
+        return logs, columns, None
+    return logs, columns, jnp.dot(
+        logs, (row <= col).astype(F32), precision=HIGHEST, preferred_element_type=F32
+    )
 
 
 def retention_states(slabs, logs, heads, key, val, spans_low):
@@ -302,14 +326,16 @@
         for p in range(halves):
             begin = lax.rem(x + p, halves) * rows
             slab_ref[pl.ds(pl.multiple_of(begin, rows), rows), :] = slab_refs[p][...]
+        all_logs, columns, _ = running_logs(log_ref, heads, blocks, False)
         for h in range(heads):
             state, total = None, None
             for n in range(blocks):
                 at = slice(n * BLOCK, (n + 1) * BLOCK)
                 k = slab_ref[at, (heads + h) * key : (heads + h + 1) * key].astype(F32)
                 v = slab_ref[at, 2 * heads * key + h * val : 2 * heads * key + (h + 1) * val]
-                logs = log_ref[h : h + 1, at]
-                c_col = running_log(logs, True)
+                i = h * blocks + n
+                logs = all_logs[i : i + 1]
+                c_col = columns[:, i : i + 1]
                 last = jnp.sum(logs, axis=1, keepdims=True)
                 kd = (k * key ** (-0.5) * jnp.exp(last - c_col)).astype(BF16)
                 u = lax.dot_general(
@@ -343,13 +369,14 @@
     per_half = rows // BLOCK
 
     def kernel(log_ref, parts_ref, before_ref, init_ref, *refs):
-        slab_refs, (out_ref, slab_ref) = refs[:halves], refs[halves:]
+        slab_refs, outs, (slab_ref, out_ref) = refs[:halves], refs[halves : 2 * halves], refs[2 * halves :]
         x, _, _, _ = place(spans_low)
         for p in range(halves):
             begin = lax.rem(x + p, halves) * rows
             slab_ref[pl.ds(pl.multiple_of(begin, rows), rows), :] = slab_refs[p][...]
         at_row = lax.broadcasted_iota(jnp.int32, (BLOCK, BLOCK), 0)
         at_col = lax.broadcasted_iota(jnp.int32, (BLOCK, BLOCK), 1)
+        all_logs, columns, lines = running_logs(log_ref, heads, halves * per_half, True)
         for h in range(heads):
             state = before_ref[h, :key] + jnp.exp(before_ref[h, key : key + 1]) * init_ref[h]
             for n in range(halves * per_half):
@@ -357,9 +384,9 @@
                 q = slab_ref[at, h * key : (h + 1) * key]
                 k = slab_ref[at, (heads + h) * key : (heads + h + 1) * key]
                 v = slab_ref[at, 2 * heads * key + h * val : 2 * heads * key + (h + 1) * val]
-                logs = log_ref[h : h + 1, at]
-                c_col = running_log(logs, True)
-                c_row = running_log(logs, False)
+                i = h * halves * per_half + n
+                logs = all_logs[i : i + 1]
+                c_col, c_row = columns[:, i : i + 1], lines[i : i + 1]
                 raw = lax.dot_general(q, k, (((1,), (1,)), ((), ())), preferred_element_type=F32)
                 gap = jnp.where(at_row >= at_col, c_col - c_row, -jnp.inf)
                 g = (raw * key ** (-0.5) * jnp.exp(gap)).astype(BF16)
@@ -376,13 +403,17 @@
                 ).astype(BF16)
                 last = jnp.sum(logs, axis=1, keepdims=True)
                 state = state * jnp.exp(last) + parts_ref[n, h]
+        for p in range(halves):
+            outs[p][...] = out_ref[p]
 
     return pl.pallas_call(
         kernel,
-        out_shape=jax.ShapeDtypeStruct((halves, rows, heads * val), BF16),
+        out_shape=[jax.ShapeDtypeStruct((rows, heads * val), BF16)] * halves,
         in_specs=whole(4 + halves),
-        out_specs=pl.BlockSpec(memory_space=VMEM),
-        scratch_shapes=[VMEM((halves * rows, width), BF16)],
+        out_specs=whole(halves),
+        scratch_shapes=[
+            VMEM((halves * rows, width), BF16), VMEM((halves, rows, heads * val), BF16)
+        ],
         cost_estimate=pl.CostEstimate(
             flops=2 * BLOCK * halves * rows * 1024, bytes_accessed=0, transcendentals=0
         ),
@@ -458,8 +489,7 @@
         own.append([send(message, spread(r)) for r, message in enumerate(messages)])
         slabs.append(slab)
     half_rows = slabs[0].shape[0]
-    w_diff = fetch(w_out_diff, slabs[0])
-    w_ret = fetch(w_out_ret, slabs[-1])
+    w_out = fetch(jnp.concatenate([w_out_diff, w_out_ret]), slabs[0])
 
     shared, packs = {}, []
     for p in range(halves):
@@ -467,8 +497,9 @@
         kv = jnp.stack([message[:2] for message in arrived])
         packs.append(kv)
         for b in range(spans_low):
-            moved = kv if b == 0 else send(kv, lambda z, y, x, c: (z, (y - b) % spans_low, x, c))
+            moved = kv
             if b:
+                moved = send(kv, lambda z, y, x, c: (z, (y - b) % spans_low, x, c))
                 shared[b, 0, p] = moved
             shared[b, 1, p] = send(moved, other_core)
     shared = [
@@ -516,18 +547,18 @@
     def product(a, w):
         return jnp.dot(a, w, preferred_element_type=F32)
 
-    w_diff = [(w, send(after(w, packs[-1]), other_core)) for w in w_diff]
-    w_ret = [(w, send(after(w, diff), other_core)) for w in w_ret]
+    outs = [
+        jnp.concatenate([b[p] for b in by_head] + [ret_out[p]], axis=1) for p in range(halves)
+    ]
+    moved = [send(outs[p], across(p)) if p else outs[p] for p in range(halves)]
+    pairs = []
+    for q, w in enumerate(w_out):
+        pairs.append((w, send(after(w, outs[-1] if q else own[-1]), other_core)))
     result = None
-    for p in reversed(range(halves)):
-        cols = jnp.concatenate([b[p] for b in by_head] + [ret_out[p]], axis=1)
-        if p:
-            cols = send(cols, across(p))
-        theirs = send(rows_of(cols, 1 - c), other_core)
-        q = (halves - p) % halves
-        split = heads * val
-        for core, rows in enumerate((rows_of(cols, c), theirs)):
-            term = product(rows[:, :split], w_diff[q][core]) + product(rows[:, split:], w_ret[q][core])
+    for p in range(halves):
+        theirs = send(rows_of(moved[p], 1 - c), other_core)
+        for core, rows in enumerate((rows_of(moved[p], c), theirs)):
+            term = product(rows, pairs[(halves - p) % halves][core])
             result = term if result is None else result + term
     return result.astype(BF16)
 

time: 99.6 us -> 100 us (level)
  local copies, waits for them, and re-layouts: 7.43 us -> 3.15 us
  starting transfers between devices: 33.1 us -> 29.2 us
  waiting for transfers between devices: 22.3 us -> 25.4 us
  other arithmetic: 1.02 us -> 3.73 us
  matrix products: 5.74 us -> 7.43 us
  Pallas kernels: 28.7 us -> 29.8 us
    unnamed x40 -> x13, local copies, waits for them, and re-layouts: 5.59 us -> 0.89 us
    ppermute x3, starting transfers between devices: 8.75 us -> 5.57 us  [on_device(): heard = lax.ppermute(local, 'sp', [(i, i ^ step) for i in range(sp)])]
    ppermute x25 -> x22, waiting for transfers between devices: 20.1 us -> 23 us  [send(): return lax.ppermute(array, axes, pairs)]
    concatenate x2, other arithmetic: 0.05 us -> 1.86 us  [on_device(): jnp.concatenate([b[p] for b in by_head] + [ret_out[p]], axis=1)]
    dot_general x8 -> x4, matrix products: 5.74 us -> 7.43 us  [product(): return jnp.dot(a, w, preferred_element_type=F32)]
    concatenate x0 -> x1, local copies, waits for them, and re-layouts: none -> 1.41 us  [on_device(): w_out = fetch(jnp.concatenate([w_out_diff, w_out_ret]), slabs[0])]
    pallas_call x1, Pallas kernels: 11.2 us -> 12.2 us  [attend(): pl.pallas_call(kernel, out_shape=[jax.ShapeDtypeStruct((halves, rows, val...]
    ppermute x25 -> x22, starting transfers between devices: 24.4 us -> 23.7 us  [send(): return lax.ppermute(array, axes, pairs)]
  transfers between devices with their start and end apart: 28 -> 25, of which waited for: 7 -> 6; matrix products, arithmetic and copies ran while one was open for 8% -> 9% of each run, Pallas kernels for 29% -> 30%
where the time goes in v1:
time: 100 us; the launch traced here: 99.2 us
  Pallas kernels  29.8 us (30%)
  starting transfers between devices  29.2 us (29%)
  waiting for transfers between devices  25.4 us (25%)
  matrix products  7.43 us (7%)
  other arithmetic  3.73 us (4%)
  local copies, waits for them, and re-layouts  3.15 us (3%)
    ppermute x22, starting transfers between devices, send(): return lax.ppermute(array, axes, pairs)  23.7 us
    ppermute x22, waiting for transfers between devices, send(): return lax.ppermute(array, axes, pairs)  23 us
    pallas_call x1, Pallas kernels, attend(): pl.pallas_call(kernel, out_shape=[jax.ShapeDtypeStruct((halves, rows, val...  12.2 us
    pallas_call x2, Pallas kernels, project(): pl.pallas_call(functools.partial(project_kernel, heads, spans_low), out_s...  11.5 us
    dot_general x4, matrix products, product(): return jnp.dot(a, w, preferred_element_type=F32)  7.43 us
    ppermute x3, starting transfers between devices, on_device(): heard = lax.ppermute(local, 'sp', [(i, i ^ step) for i in range(sp)])  5.57 us
    pallas_call x1, Pallas kernels, retain(): pl.pallas_call(kernel, out_shape=[jax.ShapeDtypeStruct((rows, heads * val...  3.5 us
    pallas_call x1, Pallas kernels, retention_states(): pl.pallas_call(kernel, out_shape=[jax.ShapeDtypeStruct((heads, key + 8, v...  2.62 us
  transfers between devices with their start and end apart: 25, of which 6 were waited for; matrix products, arithmetic and copies ran while one was open for 9% of the time, Pallas kernels for 30%

profile of v1, /device:TPU:0, one launch (start us, length us, event | category | flops | bytes accessed | tf_op | source)
XLA Modules:
  0.0 99.2 jit_solution(10742753318328915600)
XLA Ops:
  0.5 2.5 %collective-permute-start.3 = (bf16[128,2048]{1,0:T(8,128)(2,1)}, bf16[128,2048]{1,0:T(8,128)(2,1)}, u32[]{:S(2)}, u32[]{:S(2)}) collective-permute-start(bf16[128,2048]{1,0:T(8,128)(2,1)} %refs_0_.1), channel_id=1, source_target_pairs={{0,2},{1,3},{2,0},{3,1},{4,6},{5,7},{6,4},{7,5},{8,10},{9,11},{10,... | collective-permute-start | bytes 1572872 | tf_op jit(solution)/shard_map/ppermute | solution.py:443
  4.0 5.8 %project.2 = (bf16[3,256,128]{2,1,0:T(8,128)(2,1)}, bf16[3,256,128]{2,1,0:T(8,128)(2,1)}, bf16[256,512]{1,0:T(8,128)(2,1)}) custom-call(bf16[128,2048]{1,0:T(8,128)(2,1)} %refs_0_.1, bf16[128,2048]{1,0:T(8,128)(2,1)} %copy-done.3, bf16[2048,128]{1,0:T(8,128)(2,1)} %refs_2_.3, bf16[2048,128]{1,0:T(8,128)(2,1)} %refs_3_.3, bf16[2048,256]{1,0:T(8,128)(2,1)} %refs_4_.3, ...), custom_call_target="tpu_custom_call" | custom-call | flops 2147483648 | tf_op jit(solution)/shard_map/project/pallas_call | solution.py:111
  9.8 6.1 %collective-permute-done.3.refs_0_ = bf16[128,2048]{1,0:T(8,128)(2,1)} collective-permute-done((bf16[128,2048]{1,0:T(8,128)(2,1)}, bf16[128,2048]{1,0:T(8,128)(2,1)}, u32[]{:S(2)}, u32[]{:S(2)}) %collective-permute-start.3) | collective-permute-done | bytes 524320 | tf_op jit(solution)/shard_map/ppermute | solution.py:443
  16.0 1.4 %constant_dynamic-update-slice_fusion = bf16[512,2048]{1,0:T(8,128)(2,1)S(1)} fusion(bf16[512,2048]{1,0:T(8,128)(2,1)S(1)} %constant_dynamic-update-slice_fusion.1, bf16[256,2048]{1,0:T(8,128)(2,1)} %param.31), kind=kLoop, calls=%fused_computation.26 | loop fusion | bytes 2097152 | tf_op jit(solution)/shard_map/concatenate | solution.py:492
  18.1 3.6 %collective-permute-start.2 = (bf16[3,256,128]{2,1,0:T(8,128)(2,1)S(1)}, bf16[3,256,128]{2,1,0:T(8,128)(2,1)S(1)}, u32[]{:S(2)}, u32[]{:S(2)}) collective-permute-start(bf16[3,256,128]{2,1,0:T(8,128)(2,1)S(1)} %copy-done.4), channel_id=1, source_target_pairs={{0,8},{1,24},{2,10},{3,26},{4,12},{5,28},{6,14},{7,30},{8,1},{9,17... | collective-permute-start | bytes 589832 | tf_op jit(solution)/shard_map/ppermute | solution.py:443
  21.7 1.5 %collective-permute-start.22 = (bf16[512,2048]{1,0:T(8,128)(2,1)S(1)}, bf16[512,2048]{1,0:T(8,128)(2,1)}, u32[]{:S(2)}, u32[]{:S(2)}) collective-permute-start(bf16[512,2048]{1,0:T(8,128)(2,1)S(1)} %constant_dynamic-update-slice_fusion), channel_id=1, source_target_pairs={{0,2},{1,3},{2,0},{3,1},{4,6},{5,7},{6,4},{7,5},{8,10},{9,11},{10,... | collective-permute-start | bytes 6291464 | tf_op jit(solution)/shard_map/ppermute | solution.py:443
  23.2 5.7 %project.3 = (bf16[3,256,128]{2,1,0:T(8,128)(2,1)}, bf16[3,256,128]{2,1,0:T(8,128)(2,1)}, bf16[256,512]{1,0:T(8,128)(2,1)}) custom-call(bf16[128,2048]{1,0:T(8,128)(2,1)} %collective-permute-done.3.refs_0_, bf16[128,2048]{1,0:T(8,128)(2,1)} %collective-permute-done.4.refs_1_, bf16[2048,128]{1,0:T(8,128)(2,1)} %refs_2_.3, bf16[2048,128]{1,0:T(8,128)(2,1)} %refs_3_.3, ...), custom_call_target="tpu_custom_call" | custom-call | flops 2147483648 | tf_op jit(solution)/shard_map/project/pallas_call | solution.py:111
  29.0 2.3 %collective-permute-done.2.refs_1_ = bf16[3,256,128]{2,1,0:T(8,128)(2,1)S(1)} collective-permute-done((bf16[3,256,128]{2,1,0:T(8,128)(2,1)S(1)}, bf16[3,256,128]{2,1,0:T(8,128)(2,1)S(1)}, u32[]{:S(2)}, u32[]{:S(2)}) %collective-permute-start.2) | collective-permute-done | bytes 196640 | tf_op jit(solution)/shard_map/ppermute | solution.py:443
  31.3 1.7 %collective-permute-start.9 = (bf16[2,2,256,128]{3,2,1,0:T(8,128)(2,1)S(1)}, bf16[2,2,256,128]{3,2,1,0:T(8,128)(2,1)S(1)}, u32[]{:S(2)}, u32[]{:S(2)}) collective-permute-start(bf16[2,2,256,128]{3,2,1,0:T(8,128)(2,1)S(1)} %pad_maximum_fusion), channel_id=1, source_target_pairs={{0,4},{1,5},{2,6},{3,7},{4,0},{5,1},{6,2},{7,3},{8,12},{9,13},{10,... | collective-permute-start | bytes 786440 | tf_op jit(solution)/shard_map/ppermute | solution.py:443
  33.0 1.6 %collective-permute-start.5 = (bf16[3,256,128]{2,1,0:T(8,128)(2,1)}, bf16[3,256,128]{2,1,0:T(8,128)(2,1)S(1)}, u32[]{:S(2)}, u32[]{:S(2)}) collective-permute-start(bf16[3,256,128]{2,1,0:T(8,128)(2,1)} %get-tuple-element.31), channel_id=1, source_target_pairs={{0,0},{1,16},{2,2},{3,18},{4,4},{5,20},{6,6},{7,22},{8,9},{9,25},{... | collective-permute-start | bytes 589832 | tf_op jit(solution)/shard_map/ppermute | solution.py:443
  34.6 2.6 %states.1 = (f32[2,72,128]{2,1,0:T(8,128)}, f32[2,2,64,128]{3,2,1,0:T(8,128)}) custom-call(f32[2,512]{1,0:T(2,128)} %log_ref.3, bf16[256,512]{1,0:T(8,128)(2,1)} %get-tuple-element.38.refs_0_, bf16[256,512]{1,0:T(8,128)(2,1)} %get-tuple-element.39.refs_1_), custom_call_target="tpu_custom_call" | custom-call | flops 134217728 | tf_op jit(solution)/shard_map/states/pallas_call | solution.py:350
  38.4 3.3 %collective-permute-start.6 = (bf16[3,256,128]{2,1,0:T(8,128)(2,1)}, bf16[3,256,128]{2,1,0:T(8,128)(2,1)S(1)}, u32[]{:S(2)}, u32[]{:S(2)}) collective-permute-start(bf16[3,256,128]{2,1,0:T(8,128)(2,1)} %get-tuple-element.32), channel_id=1, source_target_pairs={{0,8},{1,24},{2,10},{3,26},{4,12},{5,28},{6,14},{7,30},{8,1},{9,17... | collective-permute-start | bytes 589832 | tf_op jit(solution)/shard_map/ppermute | solution.py:443
  41.7 5.5 %collective-permute-done.6.refs_3_ = bf16[3,256,128]{2,1,0:T(8,128)(2,1)S(1)} collective-permute-done((bf16[3,256,128]{2,1,0:T(8,128)(2,1)}, bf16[3,256,128]{2,1,0:T(8,128)(2,1)S(1)}, u32[]{:S(2)}, u32[]{:S(2)}) %collective-permute-start.6) | collective-permute-done | bytes 196640 | tf_op jit(solution)/shard_map/ppermute | solution.py:443
  48.2 2.4 %collective-permute-start.17 = (f32[2,72,128]{2,1,0:T(8,128)S(1)}, f32[2,72,128]{2,1,0:T(8,128)S(1)}, u32[]{:S(2)}, u32[]{:S(2)}) collective-permute-start(f32[2,72,128]{2,1,0:T(8,128)S(1)} %get-tuple-element.57), channel_id=1, source_target_pairs={{0,8},{4,12},{8,0},{12,4},{16,24},{20,28},{24,16},{28,20},{1,9},{5... | collective-permute-start | bytes 221192 | tf_op jit(solution)/shard_map/ppermute | solution.py:524
  51.2 2.5 %collective-permute-done.17 = f32[2,72,128]{2,1,0:T(8,128)S(1)} collective-permute-done((f32[2,72,128]{2,1,0:T(8,128)S(1)}, f32[2,72,128]{2,1,0:T(8,128)S(1)}, u32[]{:S(2)}, u32[]{:S(2)}) %collective-permute-start.17) | collective-permute-done | bytes 73760 | tf_op jit(solution)/shard_map/ppermute | solution.py:524
  54.6 3.4 %collective-permute-done.10.refs_7_ = bf16[2,2,256,128]{3,2,1,0:T(8,128)(2,1)S(1)} collective-permute-done((bf16[2,2,256,128]{3,2,1,0:T(8,128)(2,1)S(1)}, bf16[2,2,256,128]{3,2,1,0:T(8,128)(2,1)S(1)}, u32[]{:S(2)}, u32[]{:S(2)}) %collective-permute-start.10) | collective-permute-done | bytes 262176 | tf_op jit(solution)/shard_map/ppermute | solution.py:443
  58.8 2.7 %collective-permute-start.18 = (f32[2,72,128]{2,1,0:T(8,128)S(1)}, f32[2,72,128]{2,1,0:T(8,128)S(1)}, u32[]{:S(2)}, u32[]{:S(2)}) collective-permute-start(f32[2,72,128]{2,1,0:T(8,128)S(1)} %get-tuple-element.55), channel_id=1, source_target_pairs={{0,16},{4,20},{8,24},{12,28},{16,0},{20,4},{24,8},{28,12},{1,17},{... | collective-permute-start | bytes 221192 | tf_op jit(solution)/shard_map/ppermute | solution.py:524
  61.5 12.2 %attend.1 = (bf16[2,256,128]{2,1,0:T(8,128)(2,1)S(1)}, bf16[2,256,128]{2,1,0:T(8,128)(2,1)S(1)}) custom-call(bf16[3,256,128]{2,1,0:T(8,128)(2,1)S(1)} %collective-permute-done.1.refs_0_, bf16[3,256,128]{2,1,0:T(8,128)(2,1)S(1)} %collective-permute-done.2.refs_1_, bf16[3,256,128]{2,1,0:T(8,128)(2,1)S(1)} %collective-permute-done.5.refs_2_, ...), custom_call_target="tpu_custom_call" | custom-call | flops 4294967296 | tf_op jit(solution)/shard_map/attend/pallas_call | solution.py:276
  76.6 3.5 %retain.1 = (bf16[256,256]{1,0:T(8,128)(2,1)}, bf16[256,256]{1,0:T(8,128)(2,1)}) custom-call(f32[2,512]{1,0:T(2,128)} %log_ref.3, f32[2,2,64,128]{3,2,1,0:T(8,128)} %get-tuple-element.40.parts_ref, f32[2,72,128]{2,1,0:T(8,128)} %add_select_fusion.before_ref, f32[2,64,128]{2,1,0:T(8,128)} %init_ref.1, bf16[256,512]{1,0:T(8,128)(2,1)} %get-tuple-element.38.refs_0_, ...), custom_call_target="tpu_custom_call" | custom-call | flops 268435456 | tf_op jit(solution)/shard_map/retain/pallas_call | solution.py:409
  81.2 2.6 %collective-permute-start.24 = (bf16[512,2048]{1,0:T(8,128)(2,1)}, bf16[512,2048]{1,0:T(8,128)(2,1)}, u32[]{:S(2)}, u32[]{:S(2)}) collective-permute-start(bf16[512,2048]{1,0:T(8,128)(2,1)} %collective-permute-done.22), channel_id=1, source_target_pairs={{0,1},{1,0},{2,3},{3,2},{4,5},{5,4},{6,7},{7,6},{8,9},{9,8},{10,11... | collective-permute-start | bytes 6291464 | tf_op jit(solution)/shard_map/ppermute | solution.py:443
  86.5 5.6 %collective-permute-done.21 = bf16[256,512]{1,0:T(8,128)(2,1)S(1)} collective-permute-done((bf16[256,512]{1,0:T(8,128)(2,1)S(1)}, bf16[256,512]{1,0:T(8,128)(2,1)S(1)}, u32[]{:S(2)}, u32[]{:S(2)}) %collective-permute-start.21) | collective-permute-done | bytes 262176 | tf_op jit(solution)/shard_map/ppermute | solution.py:443
  92.2 2.1 %convolution_add_fusion.1 = f32[128,2048]{1,0:T(8,128)S(1)} fusion(f32[128,2048]{1,0:T(8,128)S(1)} %fusion.3, bf16[128,512]{1,0:T(8,128)(2,1)S(1)} %collective-permute-done.19, bf16[512,2048]{1,0:T(8,128)(2,1)} %collective-permute-done.20), kind=kOutput, calls=%fused_computation.2 | convolution fusion | flops 268697600 | bytes 4325376 | tf_op jit(solution)/shard_map/dot_general | solution.py:548
  94.3 2.1 %fusion.7 = f32[128,2048]{1,0:T(8,128)S(1)} fusion(bf16[128,512]{1,0:T(8,128)(2,1)S(1)} %collective-permute-done.23, bf16[512,2048]{1,0:T(8,128)(2,1)} %collective-permute-done.24), kind=kOutput, calls=%fused_computation.39 | convolution fusion | flops 268435456 | bytes 3276800 | tf_op jit(solution)/shard_map/dot_general | solution.py:548
  96.3 2.9 %fusion.1 = bf16[128,2048]{1,0:T(8,128)(2,1)} fusion(f32[128,2048]{1,0:T(8,128)S(1)} %fusion.7, f32[128,2048]{1,0:T(8,128)S(1)} %convolution_add_fusion.1, bf16[512,2048]{1,0:T(8,128)(2,1)} %collective-permute-done.22, bf16[256,512]{1,0:T(8,128)(2,1)S(1)} %collective-permute-done.21, s32[]{:T(128)S(6)} %select_n.118), kind=kOutput, calls=%fused_computation.3 | convolution fusion | flops 269221888 | bytes 4849668 | tf_op jit(solution)/shard_map/dot_general | solution.py:548
  (71 shorter events, 13.3 us)
Async XLA Ops:
  0.0 3.2 %collective-permute-start = (bf16[128,2048]{1,0:T(8,128)(2,1)}, bf16[128,2048]{1,0:T(8,128)(2,1)S(1)}, u32[]{:S(2)}, u32[]{:S(2)}) collective-permute-start(bf16[128,2048]{1,0:T(8,128)(2,1)} %refs_0_.1), channel_id=1, source_target_pairs={{0,1},{1,0},{2,3},{3,2},{4,5},{5,4},{6,7},{7,6},{8,9},{9,8},{10,11... | collective-permute-start | bytes 1572872 | tf_op jit(solution)/shard_map/ppermute | solution.py:443
  0.5 15.4 %collective-permute-start.3 = (bf16[128,2048]{1,0:T(8,128)(2,1)}, bf16[128,2048]{1,0:T(8,128)(2,1)}, u32[]{:S(2)}, u32[]{:S(2)}) collective-permute-start(bf16[128,2048]{1,0:T(8,128)(2,1)} %refs_0_.1), channel_id=1, source_target_pairs={{0,2},{1,3},{2,0},{3,1},{4,6},{5,7},{6,4},{7,5},{8,10},{9,11},{10,... | collective-permute-start | bytes 1572872 | tf_op jit(solution)/shard_map/ppermute | solution.py:443
  3.0 51.1 %collective-permute-start.13 = (f32[2]{0:T(128)}, f32[2]{0:T(128)S(1)}, u32[]{:S(2)}, u32[]{:S(2)}) collective-permute-start(f32[2]{0:T(128)} %refs_10_.1), channel_id=1, source_target_pairs={{0,1},{1,0},{2,3},{3,2},{4,5},{5,4},{6,7},{7,6},{8,9},{9,8},{10,11... | collective-permute-start | bytes 32 | tf_op jit(solution)/shard_map/ppermute | solution.py:443
  15.9 7.3 %collective-permute-start.4 = (bf16[128,2048]{1,0:T(8,128)(2,1)}, bf16[128,2048]{1,0:T(8,128)(2,1)}, u32[]{:S(2)}, u32[]{:S(2)}) collective-permute-start(bf16[128,2048]{1,0:T(8,128)(2,1)} %collective-permute-done.3.refs_0_), channel_id=1, source_target_pairs={{0,1},{1,0},{2,3},{3,2},{4,5},{5,4},{6,7},{7,6},{8,9},{9,8},{10,11... | collective-permute-start | bytes 1572872 | tf_op jit(solution)/shard_map/ppermute | solution.py:443
  17.4 11.6 %collective-permute-start.1 = (bf16[3,256,128]{2,1,0:T(8,128)(2,1)S(1)}, bf16[3,256,128]{2,1,0:T(8,128)(2,1)S(1)}, u32[]{:S(2)}, u32[]{:S(2)}) collective-permute-start(bf16[3,256,128]{2,1,0:T(8,128)(2,1)S(1)} %copy-done.5), channel_id=1, source_target_pairs={{0,0},{1,16},{2,2},{3,18},{4,4},{5,20},{6,6},{7,22},{8,9},{9,25},{... | collective-permute-start | bytes 589832 | tf_op jit(solution)/shard_map/ppermute | solution.py:443
  18.1 13.2 %collective-permute-start.2 = (bf16[3,256,128]{2,1,0:T(8,128)(2,1)S(1)}, bf16[3,256,128]{2,1,0:T(8,128)(2,1)S(1)}, u32[]{:S(2)}, u32[]{:S(2)}) collective-permute-start(bf16[3,256,128]{2,1,0:T(8,128)(2,1)S(1)} %copy-done.4), channel_id=1, source_target_pairs={{0,8},{1,24},{2,10},{3,26},{4,12},{5,28},{6,14},{7,30},{8,1},{9,17... | collective-permute-start | bytes 589832 | tf_op jit(solution)/shard_map/ppermute | solution.py:443
  21.7 59.4 %collective-permute-start.22 = (bf16[512,2048]{1,0:T(8,128)(2,1)S(1)}, bf16[512,2048]{1,0:T(8,128)(2,1)}, u32[]{:S(2)}, u32[]{:S(2)}) collective-permute-start(bf16[512,2048]{1,0:T(8,128)(2,1)S(1)} %constant_dynamic-update-slice_fusion), channel_id=1, source_target_pairs={{0,2},{1,3},{2,0},{3,1},{4,6},{5,7},{6,4},{7,5},{8,10},{9,11},{10,... | collective-permute-start | bytes 6291464 | tf_op jit(solution)/shard_map/ppermute | solution.py:443
  31.3 22.9 %collective-permute-start.9 = (bf16[2,2,256,128]{3,2,1,0:T(8,128)(2,1)S(1)}, bf16[2,2,256,128]{3,2,1,0:T(8,128)(2,1)S(1)}, u32[]{:S(2)}, u32[]{:S(2)}) collective-permute-start(bf16[2,2,256,128]{3,2,1,0:T(8,128)(2,1)S(1)} %pad_maximum_fusion), channel_id=1, source_target_pairs={{0,4},{1,5},{2,6},{3,7},{4,0},{5,1},{6,2},{7,3},{8,12},{9,13},{10,... | collective-permute-start | bytes 786440 | tf_op jit(solution)/shard_map/ppermute | solution.py:443
  33.0 5.4 %collective-permute-start.5 = (bf16[3,256,128]{2,1,0:T(8,128)(2,1)}, bf16[3,256,128]{2,1,0:T(8,128)(2,1)S(1)}, u32[]{:S(2)}, u32[]{:S(2)}) collective-permute-start(bf16[3,256,128]{2,1,0:T(8,128)(2,1)} %get-tuple-element.31), channel_id=1, source_target_pairs={{0,0},{1,16},{2,2},{3,18},{4,4},{5,20},{6,6},{7,22},{8,9},{9,25},{... | collective-permute-start | bytes 589832 | tf_op jit(solution)/shard_map/ppermute | solution.py:443
  37.2 10.0 %collective-permute-start.16 = (f32[2,72,128]{2,1,0:T(8,128)}, f32[2,72,128]{2,1,0:T(8,128)S(1)}, u32[]{:S(2)}, u32[]{:S(2)}) collective-permute-start(f32[2,72,128]{2,1,0:T(8,128)} %get-tuple-element.41), channel_id=1, source_target_pairs={{0,4},{4,0},{8,12},{12,8},{16,20},{20,16},{24,28},{28,24},{1,5},{5... | collective-permute-start | bytes 221192 | tf_op jit(solution)/shard_map/ppermute | solution.py:524
  38.4 8.8 %collective-permute-start.6 = (bf16[3,256,128]{2,1,0:T(8,128)(2,1)}, bf16[3,256,128]{2,1,0:T(8,128)(2,1)S(1)}, u32[]{:S(2)}, u32[]{:S(2)}) collective-permute-start(bf16[3,256,128]{2,1,0:T(8,128)(2,1)} %get-tuple-element.32), channel_id=1, source_target_pairs={{0,8},{1,24},{2,10},{3,26},{4,12},{5,28},{6,14},{7,30},{8,1},{9,17... | collective-permute-start | bytes 589832 | tf_op jit(solution)/shard_map/ppermute | solution.py:443
  48.2 5.4 %collective-permute-start.17 = (f32[2,72,128]{2,1,0:T(8,128)S(1)}, f32[2,72,128]{2,1,0:T(8,128)S(1)}, u32[]{:S(2)}, u32[]{:S(2)}) collective-permute-start(f32[2,72,128]{2,1,0:T(8,128)S(1)} %get-tuple-element.57), channel_id=1, source_target_pairs={{0,8},{4,12},{8,0},{12,4},{16,24},{20,28},{24,16},{28,20},{1,9},{5... | collective-permute-start | bytes 221192 | tf_op jit(solution)/shard_map/ppermute | solution.py:524
  50.7 7.4 %collective-permute-start.10 = (bf16[2,2,256,128]{3,2,1,0:T(8,128)(2,1)S(1)}, bf16[2,2,256,128]{3,2,1,0:T(8,128)(2,1)S(1)}, u32[]{:S(2)}, u32[]{:S(2)}) collective-permute-start(bf16[2,2,256,128]{3,2,1,0:T(8,128)(2,1)S(1)} %pad_maximum_fusion.1), channel_id=1, source_target_pairs={{0,4},{1,5},{2,6},{3,7},{4,0},{5,1},{6,2},{7,3},{8,12},{9,13},{10,... | collective-permute-start | bytes 786440 | tf_op jit(solution)/shard_map/ppermute | solution.py:443
  53.7 4.5 %collective-permute-start.7 = (bf16[2,2,256,128]{3,2,1,0:T(8,128)(2,1)S(1)}, bf16[2,2,256,128]{3,2,1,0:T(8,128)(2,1)S(1)}, u32[]{:S(2)}, u32[]{:S(2)}) collective-permute-start(bf16[2,2,256,128]{3,2,1,0:T(8,128)(2,1)S(1)} %pad_maximum_fusion), channel_id=1, source_target_pairs={{0,1},{1,0},{2,3},{3,2},{4,5},{5,4},{6,7},{7,6},{8,9},{9,8},{10,11... | collective-permute-start | bytes 786440 | tf_op jit(solution)/shard_map/ppermute | solution.py:443
  54.0 4.7 %collective-permute-start.8 = (bf16[2,2,256,128]{3,2,1,0:T(8,128)(2,1)S(1)}, bf16[2,2,256,128]{3,2,1,0:T(8,128)(2,1)S(1)}, u32[]{:S(2)}, u32[]{:S(2)}) collective-permute-start(bf16[2,2,256,128]{3,2,1,0:T(8,128)(2,1)S(1)} %pad_maximum_fusion.1), channel_id=1, source_target_pairs={{0,1},{1,0},{2,3},{3,2},{4,5},{5,4},{6,7},{7,6},{8,9},{9,8},{10,11... | collective-permute-start | bytes 786440 | tf_op jit(solution)/shard_map/ppermute | solution.py:443
  54.3 7.2 %collective-permute-start.11 = (bf16[2,2,256,128]{3,2,1,0:T(8,128)(2,1)S(1)}, bf16[2,2,256,128]{3,2,1,0:T(8,128)(2,1)S(1)}, u32[]{:S(2)}, u32[]{:S(2)}) collective-permute-start(bf16[2,2,256,128]{3,2,1,0:T(8,128)(2,1)S(1)} %collective-permute-done.9.refs_6_), channel_id=1, source_target_pairs={{0,1},{1,0},{2,3},{3,2},{4,5},{5,4},{6,7},{7,6},{8,9},{9,8},{10,11... | collective-permute-start | bytes 786440 | tf_op jit(solution)/shard_map/ppermute | solution.py:443
  58.0 3.4 %collective-permute-start.12 = (bf16[2,2,256,128]{3,2,1,0:T(8,128)(2,1)S(1)}, bf16[2,2,256,128]{3,2,1,0:T(8,128)(2,1)S(1)}, u32[]{:S(2)}, u32[]{:S(2)}) collective-permute-start(bf16[2,2,256,128]{3,2,1,0:T(8,128)(2,1)S(1)} %collective-permute-done.10.refs_7_), channel_id=1, source_target_pairs={{0,1},{1,0},{2,3},{3,2},{4,5},{5,4},{6,7},{7,6},{8,9},{9,8},{10,11... | collective-permute-start | bytes 786440 | tf_op jit(solution)/shard_map/ppermute | solution.py:443
  58.2 34.0 %collective-permute-start.20 = (bf16[512,2048]{1,0:T(8,128)(2,1)S(1)}, bf16[512,2048]{1,0:T(8,128)(2,1)}, u32[]{:S(2)}, u32[]{:S(2)}) collective-permute-start(bf16[512,2048]{1,0:T(8,128)(2,1)S(1)} %constant_dynamic-update-slice_fusion), channel_id=1, source_target_pairs={{0,1},{1,0},{2,3},{3,2},{4,5},{5,4},{6,7},{7,6},{8,9},{9,8},{10,11... | collective-permute-start | bytes 6291464 | tf_op jit(solution)/shard_map/ppermute | solution.py:443
  58.8 17.1 %collective-permute-start.18 = (f32[2,72,128]{2,1,0:T(8,128)S(1)}, f32[2,72,128]{2,1,0:T(8,128)S(1)}, u32[]{:S(2)}, u32[]{:S(2)}) collective-permute-start(f32[2,72,128]{2,1,0:T(8,128)S(1)} %get-tuple-element.55), channel_id=1, source_target_pairs={{0,16},{4,20},{8,24},{12,28},{16,0},{20,4},{24,8},{28,12},{1,17},{... | collective-permute-start | bytes 221192 | tf_op jit(solution)/shard_map/ppermute | solution.py:524
  73.7 6.4 %collective-permute-start.14 = (bf16[2,256,128]{2,1,0:T(8,128)(2,1)S(1)}, bf16[2,256,128]{2,1,0:T(8,128)(2,1)S(1)}, u32[]{:S(2)}, u32[]{:S(2)}) collective-permute-start(bf16[2,256,128]{2,1,0:T(8,128)(2,1)S(1)} %get-tuple-element.36), channel_id=1, source_target_pairs={{0,24},{1,8},{2,26},{3,10},{4,28},{5,12},{6,30},{7,14},{8,0},{9,16... | collective-permute-start | bytes 393224 | tf_op jit(solution)/shard_map/ppermute | solution.py:443
  75.1 5.1 %collective-permute-start.15 = (bf16[2,256,128]{2,1,0:T(8,128)(2,1)S(1)}, bf16[2,256,128]{2,1,0:T(8,128)(2,1)S(1)}, u32[]{:S(2)}, u32[]{:S(2)}) collective-permute-start(bf16[2,256,128]{2,1,0:T(8,128)(2,1)S(1)} %get-tuple-element.37), channel_id=1, source_target_pairs={{0,0},{1,16},{2,2},{3,18},{4,4},{5,20},{6,6},{7,22},{8,24},{9,8},{... | collective-permute-start | bytes 393224 | tf_op jit(solution)/shard_map/ppermute | solution.py:443
  81.2 13.1 %collective-permute-start.24 = (bf16[512,2048]{1,0:T(8,128)(2,1)}, bf16[512,2048]{1,0:T(8,128)(2,1)}, u32[]{:S(2)}, u32[]{:S(2)}) collective-permute-start(bf16[512,2048]{1,0:T(8,128)(2,1)} %collective-permute-done.22), channel_id=1, source_target_pairs={{0,1},{1,0},{2,3},{3,2},{4,5},{5,4},{6,7},{7,6},{8,9},{9,8},{10,11... | collective-permute-start | bytes 6291464 | tf_op jit(solution)/shard_map/ppermute | solution.py:443
  83.7 8.3 %collective-permute-start.21 = (bf16[256,512]{1,0:T(8,128)(2,1)S(1)}, bf16[256,512]{1,0:T(8,128)(2,1)S(1)}, u32[]{:S(2)}, u32[]{:S(2)}) collective-permute-start(bf16[256,512]{1,0:T(8,128)(2,1)S(1)} %pad_maximum_fusion.3), channel_id=1, source_target_pairs={{0,2},{1,3},{2,0},{3,1},{4,6},{5,7},{6,4},{7,5},{8,10},{9,11},{10,... | collective-permute-start | bytes 786440 | tf_op jit(solution)/shard_map/ppermute | solution.py:443
  85.9 6.2 %collective-permute-start.19 = (bf16[128,512]{1,0:T(8,128)(2,1)S(1)}, bf16[128,512]{1,0:T(8,128)(2,1)S(1)}, u32[]{:S(2)}, u32[]{:S(2)}) collective-permute-start(bf16[128,512]{1,0:T(8,128)(2,1)S(1)} %constant_dynamic-slice_fusion.1), channel_id=1, source_target_pairs={{0,1},{1,0},{2,3},{3,2},{4,5},{5,4},{6,7},{7,6},{8,9},{9,8},{10,11... | collective-permute-start | bytes 393224 | tf_op jit(solution)/shard_map/ppermute | solution.py:443
  (7 other events, 83.6 us)
